TPU v7x, 768 devices: a whole 4x8x12 slice. The times are simulated.
768 devices in a mesh: ep: 24 (over z, core), tp: 32 (over y, x).
Axes of the slice: x: 4, y: 8, z: 12, core: 2. Of those that a mesh axis runs over, the one named last changes fastest.
Arguments:
- hidden: bfloat16 [384, 4096], P('ep', 'tp'), may hold values from -6 to 6
- norm_gain: float32 [4096], replicated, may hold values from 0.1 to 1.9
- routes: int32 [384, 4], P('ep'), may hold values from 0 to 47, all different within a row; in each aligned block of 16 rows (0 to 15, 16 to 31, ...) at most 3 rows name the same one
- route_weights: float32 [384, 4], P('ep'), may hold values from 0.1 to 1
- gate_weight: bfloat16 [48, 1024, 4096], P('ep', 'tp'), may hold values from -0.09375 to 0.09375
- up_weight: bfloat16 [48, 1024, 4096], P('ep', 'tp'), may hold values from -0.09375 to 0.09375
- down_weight: bfloat16 [48, 1024, 4096], P('ep', 'tp'), may hold values from -0.375 to 0.375
- shared_gate: bfloat16 [1024, 4096], P('tp'), may hold values from -0.09375 to 0.09375
- shared_up: bfloat16 [1024, 4096], P('tp'), may hold values from -0.09375 to 0.09375
- shared_down: bfloat16 [1024, 4096], P('tp'), may hold values from -0.375 to 0.375
Outputs:
- mixed: bfloat16 [384, 4096], P('ep', 'tp')
Inputs may be any that keep to these rules, and one draw needn't show every extreme that they name: `routes`: each row names 4 different experts; among the rows of one index of ep (aligned blocks of 16 rows) no expert is named more than 3 times, a bound that some block reaches.
All inputs are finite; a program needn't handle non-finite values.
Results may differ from a plain program's by a relative error of at most 0.017.
Values may be sent and summed in bfloat16 or wider, within the bound.
No kernel may reach another device: no remote copies, remote signals or barrier semaphores. Data moves between devices by JAX's collectives and lax.ppermute only.
A program may use at most 64 MiB of HBM per device.

v0:
```python
import jax
import jax.numpy as jnp
from jax import lax
from jax.experimental import pallas as pl
from jax.experimental.pallas import tpu as pltpu
from jax.sharding import Mesh, PartitionSpec as P

norm_eps = 1e-06
f32 = jnp.float32
bf16 = jnp.bfloat16

N_Z, N_C, N_Y, N_X = 12, 2, 8, 4
N_TP = N_Y * N_X
N_Q = 4
RANKS = 4
CAP = 3
TOK = 16
LOCAL = N_Q * RANKS
SLOTS = N_Z * LOCAL
ROWS = 40
ALL = ROWS + TOK
LANES = 128
HALF = 2048
UNITS = 32


def expert_of(j):
    return 2 * ((j // N_X) % 2) + j % 2


def iota(shape, dim):
    return lax.broadcasted_iota(jnp.int32, shape, dim)


def dot(a, b, dims, precision=None):
    return lax.dot_general(a, b, (dims, ((), ())), preferred_element_type=f32, precision=precision)


def pack_body(routes_ref, hidden_ref, out_ref):
    slot = iota((SLOTS, TOK), 0)
    named = jnp.zeros((SLOTS, TOK), f32)
    for k in range(4):
        named = named + jnp.where(routes_ref[k : k + 1, :] == slot // RANKS, 1.0, 0.0)
    earlier = jnp.where(iota((TOK, TOK), 0) < iota((TOK, TOK), 1), 1.0, 0.0)
    rank = dot(named.astype(bf16), earlier.astype(bf16), ((1,), (0,)))
    select = jnp.where(rank == (slot % RANKS).astype(f32), named, 0.0)
    out_ref[...] = dot(select.astype(bf16), hidden_ref[...], ((1,), (0,))).astype(bf16)


def combine_body(routes_ref, weights_ref, out_ref):
    slot = iota((TOK, SLOTS), 1)
    hits = [routes_ref[:, k : k + 1] == slot // RANKS for k in range(4)]
    named = sum(jnp.where(hit, 1.0, 0.0) for hit in hits)
    earlier = jnp.where(iota((TOK, TOK), 1) < iota((TOK, TOK), 0), 1.0, 0.0)
    rank = dot(earlier.astype(bf16), named.astype(bf16), ((1,), (0,)))
    here = rank == (slot % RANKS).astype(f32)
    total = sum(jnp.where(hits[k], weights_ref[:, k : k + 1], 0.0) for k in range(4))
    out_ref[...] = jnp.where(here, total, 0.0)


def slot_match(shape, slot_dim, row_dim):
    slot = iota(shape, slot_dim)
    row = iota(shape, row_dim)
    rank = slot % RANKS
    target = ((slot // RANKS) % N_Q) * ROWS + (slot // LOCAL) * CAP + rank
    return jnp.where((row == target) & (rank < CAP), 1.0, 0.0).astype(bf16)


def spread_body(arrived_ref, hidden_ref, out_ref):
    match = slot_match((N_Q * ROWS, SLOTS), 1, 0)
    rows = dot(match, arrived_ref[...], ((1,), (0,))).astype(bf16)
    own = hidden_ref[...]
    for j in range(N_TP):
        q = expert_of(j)
        out_ref[j, 0:ROWS, :] = rows[q * ROWS : (q + 1) * ROWS]
        out_ref[j, ROWS:ALL, :] = own


def weights_body(pos_ref, gate_ref, up_ref, down_ref, o0, o1, o2, o3, sems):
    copies = []
    for m, out in enumerate((o0, o1, o2, o3)):
        v = pos_ref[m]
        for w, ref in enumerate((gate_ref, up_ref, down_ref)):
            copy = pltpu.make_async_copy(
                ref.at[v % 2, :, pl.ds((v // 2) * HALF, HALF)], out.at[w], sems.at[m, w]
            )
            copy.start()
            copies.append(copy)
    for copy in copies:
        copy.wait()


def silu(v):
    return v / (1.0 + jnp.exp(-v))


def experts_body(core_ref, rows_ref, gain_ref, sg, su, sd, *refs):
    given, (out_ref, normed, held, sems) = refs[:8], refs[8:]
    copies = [pltpu.make_async_copy(given[i], held.at[i], sems.at[i]) for i in range(8)]
    for copy in copies:
        copy.start()
    core = core_ref[0]
    squares = jnp.zeros((ALL, LANES), f32)
    for s in range(N_TP):
        v = rows_ref[s].astype(f32)
        squares = squares + v * v
    inv = lax.rsqrt(jnp.sum(squares, axis=1, keepdims=True) * (1.0 / (N_TP * LANES)) + norm_eps)
    for s in range(N_TP):
        normed[s] = (rows_ref[s].astype(f32) * inv * gain_ref[s]).astype(bf16)
    mine = (0, 1, 2, 3)
    other = (6, 7, 4, 5)
    nt = ((1,), (1,))

    def wide(first):
        return jnp.concatenate([normed[first + s] for s in range(N_TP // 2)], axis=1)

    x_mine = wide(core * (N_TP // 2))
    x_other = wide((1 - core) * (N_TP // 2))

    for copy in copies:
        copy.wait()

    def project(w):
        w_mine = jnp.concatenate([held[i, w] for i in mine], axis=0)
        w_other = jnp.concatenate([held[i, w] for i in other], axis=0)
        return dot(x_mine[0:ROWS], w_mine, nt) + dot(x_other[0:ROWS], w_other, nt)

    inner = (silu(project(0)) * project(1)).astype(bf16)
    x_own = jnp.concatenate([normed[s, ROWS:ALL, :] for s in range(N_TP)], axis=1)
    shared = (silu(dot(x_own, sg[...], nt)) * dot(x_own, su[...], nt)).astype(bf16)
    nn = ((1,), (0,))
    for side, slots in ((core, mine), (1 - core, other)):
        w = jnp.concatenate([held[i, 2] for i in slots], axis=0)
        part = dot(inner, w, nn).astype(bf16)
        for s in range(N_TP // 2):
            out_ref[side * (N_TP // 2) + s, 0:ROWS, :] = part[:, s * LANES : (s + 1) * LANES]
    part = dot(shared, sd[...], nn).astype(bf16)
    for s in range(N_TP):
        out_ref[s, ROWS:ALL, :] = part[:, s * LANES : (s + 1) * LANES]


def sum_body(parts_ref, out_ref, shared_ref):
    sums = []
    for q in range(N_Q):
        total = jnp.zeros((ROWS, LANES), f32)
        for s in range(N_TP):
            if expert_of(s) == q:
                total = total + parts_ref[s, 0:ROWS, :].astype(f32)
        sums.append(total.astype(bf16))
    match = slot_match((SLOTS, N_Q * ROWS), 0, 1)
    out_ref[...] = dot(match, jnp.concatenate(sums, axis=0), ((1,), (0,))).astype(bf16)
    shared = jnp.zeros((TOK, LANES), f32)
    for s in range(N_TP):
        shared = shared + parts_ref[s, ROWS:ALL, :].astype(f32)
    shared_ref[...] = shared


def final_body(combine_ref, returned_ref, shared_ref, out_ref):
    routed = dot(
        combine_ref[...], returned_ref[...].astype(f32), ((1,), (0,)), lax.Precision.HIGHEST
    )
    out_ref[...] = (routed + shared_ref[...]).astype(bf16)


VMEM = pl.BlockSpec(memory_space=pltpu.VMEM)
SMEM = pl.BlockSpec(memory_space=pltpu.SMEM)
ANY = pl.BlockSpec(memory_space=pl.ANY)


def call(body, ins, outs, *args, scratch=(), limit=4):
    single = not isinstance(outs, list)
    shapes = [outs] if single else outs
    spaces = {id(VMEM): pltpu.VMEM, id(ANY): pltpu.HBM}
    args = [
        pltpu.with_memory_space_constraint(arg, spaces[id(spec)]) if id(spec) in spaces else arg
        for spec, arg in zip(ins, args, strict=True)
    ]
    got = pl.pallas_call(
        body,
        in_specs=ins,
        out_specs=[VMEM] * len(shapes),
        out_shape=shapes,
        scratch_shapes=list(scratch),
        compiler_params=pltpu.CompilerParams(vmem_limit_bytes=limit << 20),
    )(*args)
    return got[0] if single else got


def shape(dims, dtype=bf16):
    return pltpu.VMEM(dims, dtype)


def per_device(
    hidden,
    norm_gain,
    routes,
    route_weights,
    gate_weight,
    up_weight,
    down_weight,
    shared_gate,
    shared_up,
    shared_down,
):
    core, y, x = lax.axis_index("c"), lax.axis_index("y"), lax.axis_index("x")
    place = 2 * (y % 2) + x % 2
    packed = call(pack_body, [VMEM] * 2, shape((SLOTS, LANES)), routes.T, hidden)
    arrived = lax.all_to_all(packed.reshape(N_Z, LOCAL, LANES), "z", 0, 0, tiled=True)
    order = jnp.bitwise_xor(place, jnp.arange(4, dtype=jnp.int32))
    pieces = call(
        weights_body,
        [SMEM, ANY, ANY, ANY],
        [shape((3, UNITS, HALF))] * 4,
        order,
        gate_weight,
        up_weight,
        down_weight,
        scratch=[pltpu.SemaphoreType.DMA((4, 3))],
    )
    mine = []
    for m, piece in enumerate(pieces):
        pairs = []
        for c in range(N_C):
            for j in range(N_TP):
                sy, sx = j // N_X, j % N_X
                v = (2 * (sy % 2) + sx % 2) ^ m
                target = (v // 2) * N_TP + (sy - sy % 2 + c) * N_X + (sx - sx % 2 + v % 2)
                pairs.append((c * N_TP + j, target))
        mine.append(lax.ppermute(piece, ("c", "y", "x"), pairs))
    other = []
    for piece in mine:
        other.append(lax.ppermute(piece, "c", [(0, 1), (1, 0)]))
    combine = call(combine_body, [VMEM] * 2, shape((TOK, SLOTS), f32), routes, route_weights)
    spread = call(
        spread_body, [VMEM] * 2, shape((N_TP, ALL, LANES)), arrived.reshape(SLOTS, LANES), hidden
    )
    rows = lax.all_to_all(spread, ("y", "x"), 0, 0, tiled=True)
    parts = call(
        experts_body,
        [SMEM] + [VMEM] * 5 + [ANY] * 8,
        shape((N_TP, ALL, LANES)),
        core.reshape(1).astype(jnp.int32),
        rows,
        norm_gain.reshape(N_TP, 1, LANES),
        shared_gate,
        shared_up,
        shared_down,
        *mine,
        *other,
        scratch=[
            pltpu.VMEM((N_TP, ALL, LANES), bf16),
            pltpu.VMEM((8, 3, UNITS, HALF), bf16),
            pltpu.SemaphoreType.DMA((8,)),
        ],
        limit=24,
    )
    parts = lax.all_to_all(parts, ("y", "x"), 0, 0, tiled=True)
    answers, shared_sum = call(
        sum_body, [VMEM], [shape((SLOTS, LANES)), shape((TOK, LANES), f32)], parts
    )
    returned = lax.all_to_all(answers.reshape(N_Z, LOCAL, LANES), "z", 0, 0, tiled=True)
    return call(
        final_body, [VMEM] * 3, shape((TOK, LANES)), combine, returned.reshape(SLOTS, LANES), shared_sum
    )


def solution(mesh):
    fine = Mesh(mesh.devices.reshape(N_Z, N_C, N_Y, N_X), ("z", "c", "y", "x"))
    ep, tp = ("z", "c"), ("y", "x")
    in_specs = (
        P(ep, tp),
        P(),
        P(ep, None),
        P(ep, None),
        P(ep, tp, None),
        P(ep, tp, None),
        P(ep, tp, None),
        P(tp, None),
        P(tp, None),
        P(tp, None),
    )

    return jax.shard_map(
        per_device, mesh=fine, in_specs=in_specs, out_specs=P(ep, tp), check_vma=False
    )
```

profile of v0, /device:TPU:1, one launch (start us, length us, event | category | flops | bytes accessed | tf_op | source)
XLA Modules:
  0.0 113.5 jit_solution(3602307928886632799)
XLA Ops:
  0.0 0.7 copy-done.4
  0.7 0.7 copy-done.6
  1.4 0.9 shard_map.101
  2.3 15.7 %all-to-all-start = ((bf16[12,16,128]{2,1,0:T(8,128)(2,1)}), bf16[12,16,128]{2,1,0:T(8,128)(2,1)S(1)}, u32[]{:S(2)}, u32[]{:S(2)}) async-start(bf16[12,16,128]{2,1,0:T(8,128)(2,1)} %bitcast.2), calls=%async_computation | async-start | bytes 98304 | tf_op jit(solution)/shard_map/all_to_all | solution.py:208
  18.0 9.7 %all-to-all-done = bf16[12,16,128]{2,1,0:T(8,128)(2,1)S(1)} async-done(((bf16[12,16,128]{2,1,0:T(8,128)(2,1)}), bf16[12,16,128]{2,1,0:T(8,128)(2,1)S(1)}, u32[]{:S(2)}, u32[]{:S(2)}) %all-to-all-start) | async-done | bytes 49184 | tf_op jit(solution)/shard_map/all_to_all | solution.py:208
  27.6 1.0 shard_map.102
  28.6 9.7 %all-to-all-start.1 = ((bf16[32,56,128]{2,1,0:T(8,128)(2,1)}), bf16[32,56,128]{2,1,0:T(8,128)(2,1)S(1)}, u32[]{:S(2)}, u32[]{:S(2)}) async-start(bf16[32,56,128]{2,1,0:T(8,128)(2,1)} %shard_map.102), calls=%async_computation.1 | async-start | bytes 917504 | tf_op jit(solution)/shard_map/all_to_all | solution.py:237
  38.3 2.1 %shard_map.103 = (bf16[3,32,2048]{2,1,0:T(8,128)(2,1)S(1)}, bf16[3,32,2048]{2,1,0:T(8,128)(2,1)S(1)}, bf16[3,32,2048]{2,1,0:T(8,128)(2,1)S(1)}, bf16[3,32,2048]{2,1,0:T(8,128)(2,1)S(1)}) custom-call(s32[4]{0:T(128)S(1)} %iota_xor_fusion.pos_ref, bf16[2,32,4096]{2,1,0:T(8,128)(2,1)} %gate_ref.1, bf16[2,32,4096]{2,1,0:T(8,128)(2,1)} %up_ref.1, ...), custom_call_target="tpu_custom_call" | custom-call | tf_op jit(solution)/shard_map/pallas_call | solution.py:178
  40.5 5.7 %collective-permute-start = (bf16[3,32,2048]{2,1,0:T(8,128)(2,1)S(1)}, bf16[3,32,2048]{2,1,0:T(8,128)(2,1)S(1)}, u32[]{:S(2)}, u32[]{:S(2)}) collective-permute-start(bf16[3,32,2048]{2,1,0:T(8,128)(2,1)S(1)} %get-tuple-element.11), channel_id=1, source_target_pairs={{0,0},{1,1},{2,2},{3,3},{4,32},{5,33},{6,34},{7,35},{8,8},{9,9},{1... | collective-permute-start | bytes 1179656 | tf_op jit(solution)/shard_map/ppermute | solution.py:229
  46.1 2.8 %collective-permute-start.1 = (bf16[3,32,2048]{2,1,0:T(8,128)(2,1)S(1)}, bf16[3,32,2048]{2,1,0:T(8,128)(2,1)S(1)}, u32[]{:S(2)}, u32[]{:S(2)}) collective-permute-start(bf16[3,32,2048]{2,1,0:T(8,128)(2,1)S(1)} %get-tuple-element.12), channel_id=1, source_target_pairs={{0,1},{1,0},{2,3},{3,2},{4,33},{5,32},{6,35},{7,34},{8,9},{9,8},{1... | collective-permute-start | bytes 1179656 | tf_op jit(solution)/shard_map/ppermute | solution.py:229
  49.0 1.9 %collective-permute-start.2 = (bf16[3,32,2048]{2,1,0:T(8,128)(2,1)S(1)}, bf16[3,32,2048]{2,1,0:T(8,128)(2,1)S(1)}, u32[]{:S(2)}, u32[]{:S(2)}) collective-permute-start(bf16[3,32,2048]{2,1,0:T(8,128)(2,1)S(1)} %get-tuple-element.13), channel_id=1, source_target_pairs={{0,32},{1,33},{2,34},{3,35},{4,0},{5,1},{6,2},{7,3},{8,40},{9,41},... | collective-permute-start | bytes 1179656 | tf_op jit(solution)/shard_map/ppermute | solution.py:229
  50.9 3.7 %collective-permute-start.3 = (bf16[3,32,2048]{2,1,0:T(8,128)(2,1)S(1)}, bf16[3,32,2048]{2,1,0:T(8,128)(2,1)S(1)}, u32[]{:S(2)}, u32[]{:S(2)}) collective-permute-start(bf16[3,32,2048]{2,1,0:T(8,128)(2,1)S(1)} %get-tuple-element.14), channel_id=1, source_target_pairs={{0,33},{1,32},{2,35},{3,34},{4,1},{5,0},{6,3},{7,2},{8,41},{9,40},... | collective-permute-start | bytes 1179656 | tf_op jit(solution)/shard_map/ppermute | solution.py:229
  54.9 1.9 %collective-permute-start.4 = (bf16[3,32,2048]{2,1,0:T(8,128)(2,1)S(1)}, bf16[3,32,2048]{2,1,0:T(8,128)(2,1)S(1)}, u32[]{:S(2)}, u32[]{:S(2)}) collective-permute-start(bf16[3,32,2048]{2,1,0:T(8,128)(2,1)S(1)} %collective-permute-done.refs_0_), channel_id=1, source_target_pairs={{0,32},{32,0},{1,33},{33,1},{2,34},{34,2},{3,35},{35,3},{4,36},{36... | collective-permute-start | bytes 1179656 | tf_op jit(solution)/shard_map/ppermute | solution.py:232
  56.8 3.0 %collective-permute-done.1.refs_1_ = bf16[3,32,2048]{2,1,0:T(8,128)(2,1)S(1)} collective-permute-done((bf16[3,32,2048]{2,1,0:T(8,128)(2,1)S(1)}, bf16[3,32,2048]{2,1,0:T(8,128)(2,1)S(1)}, u32[]{:S(2)}, u32[]{:S(2)}) %collective-permute-start.1) | collective-permute-done | bytes 393248 | tf_op jit(solution)/shard_map/ppermute | solution.py:229
  59.8 1.9 %collective-permute-start.5 = (bf16[3,32,2048]{2,1,0:T(8,128)(2,1)S(1)}, bf16[3,32,2048]{2,1,0:T(8,128)(2,1)}, u32[]{:S(2)}, u32[]{:S(2)}) collective-permute-start(bf16[3,32,2048]{2,1,0:T(8,128)(2,1)S(1)} %collective-permute-done.1.refs_1_), channel_id=1, source_target_pairs={{0,32},{32,0},{1,33},{33,1},{2,34},{34,2},{3,35},{35,3},{4,36},{36... | collective-permute-start | bytes 1179656 | tf_op jit(solution)/shard_map/ppermute | solution.py:232
  61.8 3.9 %collective-permute-start.6 = (bf16[3,32,2048]{2,1,0:T(8,128)(2,1)S(1)}, bf16[3,32,2048]{2,1,0:T(8,128)(2,1)}, u32[]{:S(2)}, u32[]{:S(2)}) collective-permute-start(bf16[3,32,2048]{2,1,0:T(8,128)(2,1)S(1)} %collective-permute-done.2.refs_2_), channel_id=1, source_target_pairs={{0,32},{32,0},{1,33},{33,1},{2,34},{34,2},{3,35},{35,3},{4,36},{36... | collective-permute-start | bytes 1179656 | tf_op jit(solution)/shard_map/ppermute | solution.py:232
  65.7 5.1 %collective-permute-start.7 = (bf16[3,32,2048]{2,1,0:T(8,128)(2,1)S(1)}, bf16[3,32,2048]{2,1,0:T(8,128)(2,1)}, u32[]{:S(2)}, u32[]{:S(2)}) collective-permute-start(bf16[3,32,2048]{2,1,0:T(8,128)(2,1)S(1)} %collective-permute-done.3.refs_3_), channel_id=1, source_target_pairs={{0,32},{32,0},{1,33},{33,1},{2,34},{34,2},{3,35},{35,3},{4,36},{36... | collective-permute-start | bytes 1179656 | tf_op jit(solution)/shard_map/ppermute | solution.py:232
  70.8 1.4 %collective-permute-done.7.refs_7_ = bf16[3,32,2048]{2,1,0:T(8,128)(2,1)} collective-permute-done((bf16[3,32,2048]{2,1,0:T(8,128)(2,1)S(1)}, bf16[3,32,2048]{2,1,0:T(8,128)(2,1)}, u32[]{:S(2)}, u32[]{:S(2)}) %collective-permute-start.7) | collective-permute-done | bytes 393248 | tf_op jit(solution)/shard_map/ppermute | solution.py:232
  72.3 3.1 %shard_map.104 = bf16[32,56,128]{2,1,0:T(8,128)(2,1)S(1)} custom-call(s32[1]{0:T(128)} %bitcast.core_ref, bf16[32,56,128]{2,1,0:T(8,128)(2,1)S(1)} %all-to-all-done.1.rows_ref, f32[32,1,128]{2,1,0:T(1,128)S(1)} %bitcast.9, bf16[32,4096]{1,0:T(8,128)(2,1)S(1)} %copy-done, bf16[32,4096]{1,0:T(8,128)(2,1)S(1)} %copy-done.1, bf16[32,4096]{1,0:T(8,128)(2,1)S(1)} %copy-done.2, ...), custom_call_target="tpu_custom_call" | custom-call | tf_op jit(solution)/shard_map/pallas_call | solution.py:178
  75.4 23.3 %all_to_all.20.parts_ref = bf16[32,56,128]{2,1,0:T(8,128)(2,1)S(1)} all-to-all(bf16[32,56,128]{2,1,0:T(8,128)(2,1)S(1)} %shard_map.104), channel_id=1, replica_groups=mesh['z'=12,'c'=2,'y'=8,'x'=4] {'y','x'}, dimensions={0} | all-to-all | bytes 917504 | tf_op jit(solution)/shard_map/all_to_all | solution.py:257
  98.7 0.8 shard_map.105
  99.5 3.6 %all-to-all-start.3 = ((bf16[12,16,128]{2,1,0:T(8,128)(2,1)}), bf16[12,16,128]{2,1,0:T(8,128)(2,1)S(1)}, u32[]{:S(2)}, u32[]{:S(2)}) async-start(bf16[12,16,128]{2,1,0:T(8,128)(2,1)} %bitcast.5), calls=%async_computation.3 | async-start | bytes 98304 | tf_op jit(solution)/shard_map/all_to_all | solution.py:261
  104.1 8.6 %all-to-all-done.3 = bf16[12,16,128]{2,1,0:T(8,128)(2,1)S(1)} async-done(((bf16[12,16,128]{2,1,0:T(8,128)(2,1)}), bf16[12,16,128]{2,1,0:T(8,128)(2,1)S(1)}, u32[]{:S(2)}, u32[]{:S(2)}) %all-to-all-start.3) | async-done | bytes 49184 | tf_op jit(solution)/shard_map/all_to_all | solution.py:261
  112.9 0.6 copy.13
  (38 shorter events, 1.5 us)
Async XLA Ops:
  0.0 0.7 copy-start.4
  2.3 25.4 %all-to-all-start = ((bf16[12,16,128]{2,1,0:T(8,128)(2,1)}), bf16[12,16,128]{2,1,0:T(8,128)(2,1)S(1)}, u32[]{:S(2)}, u32[]{:S(2)}) async-start(bf16[12,16,128]{2,1,0:T(8,128)(2,1)} %bitcast.2), calls=%async_computation | async-start | bytes 98304 | tf_op jit(solution)/shard_map/all_to_all | solution.py:208
  18.0 9.7 %copy-start.5 = (bf16[16,128]{1,0:T(8,128)(2,1)S(1)}, bf16[16,128]{1,0:T(8,128)(2,1)}, u32[]{:S(2)}) copy-start(bf16[16,128]{1,0:T(8,128)(2,1)} %hidden_ref.3) | copy-start | bytes 12292
  28.6 43.6 %all-to-all-start.1 = ((bf16[32,56,128]{2,1,0:T(8,128)(2,1)}), bf16[32,56,128]{2,1,0:T(8,128)(2,1)S(1)}, u32[]{:S(2)}, u32[]{:S(2)}) async-start(bf16[32,56,128]{2,1,0:T(8,128)(2,1)} %shard_map.102), calls=%async_computation.1 | async-start | bytes 917504 | tf_op jit(solution)/shard_map/all_to_all | solution.py:237
  38.3 34.0 %copy-start = (bf16[32,4096]{1,0:T(8,128)(2,1)S(1)}, bf16[32,4096]{1,0:T(8,128)(2,1)}, u32[]{:S(2)}) copy-start(bf16[32,4096]{1,0:T(8,128)(2,1)} %sg.1) | copy-start | bytes 786436
  38.3 34.0 %copy-start.1 = (bf16[32,4096]{1,0:T(8,128)(2,1)S(1)}, bf16[32,4096]{1,0:T(8,128)(2,1)}, u32[]{:S(2)}) copy-start(bf16[32,4096]{1,0:T(8,128)(2,1)} %su.1) | copy-start | bytes 786436
  38.3 34.0 %copy-start.2 = (bf16[32,4096]{1,0:T(8,128)(2,1)S(1)}, bf16[32,4096]{1,0:T(8,128)(2,1)}, u32[]{:S(2)}) copy-start(bf16[32,4096]{1,0:T(8,128)(2,1)} %sd.1) | copy-start | bytes 786436
  40.4 31.9 %copy-start.3 = (f32[4096]{0:T(1024)S(1)}, f32[4096]{0:T(1024)}, u32[]{:S(2)}) copy-start(f32[4096]{0:T(1024)} %param.11) | copy-start | bytes 49156
  40.5 14.4 %collective-permute-start = (bf16[3,32,2048]{2,1,0:T(8,128)(2,1)S(1)}, bf16[3,32,2048]{2,1,0:T(8,128)(2,1)S(1)}, u32[]{:S(2)}, u32[]{:S(2)}) collective-permute-start(bf16[3,32,2048]{2,1,0:T(8,128)(2,1)S(1)} %get-tuple-element.11), channel_id=1, source_target_pairs={{0,0},{1,1},{2,2},{3,3},{4,32},{5,33},{6,34},{7,35},{8,8},{9,9},{1... | collective-permute-start | bytes 1179656 | tf_op jit(solution)/shard_map/ppermute | solution.py:229
  46.1 13.7 %collective-permute-start.1 = (bf16[3,32,2048]{2,1,0:T(8,128)(2,1)S(1)}, bf16[3,32,2048]{2,1,0:T(8,128)(2,1)S(1)}, u32[]{:S(2)}, u32[]{:S(2)}) collective-permute-start(bf16[3,32,2048]{2,1,0:T(8,128)(2,1)S(1)} %get-tuple-element.12), channel_id=1, source_target_pairs={{0,1},{1,0},{2,3},{3,2},{4,33},{5,32},{6,35},{7,34},{8,9},{9,8},{1... | collective-permute-start | bytes 1179656 | tf_op jit(solution)/shard_map/ppermute | solution.py:229
  49.0 12.8 %collective-permute-start.2 = (bf16[3,32,2048]{2,1,0:T(8,128)(2,1)S(1)}, bf16[3,32,2048]{2,1,0:T(8,128)(2,1)S(1)}, u32[]{:S(2)}, u32[]{:S(2)}) collective-permute-start(bf16[3,32,2048]{2,1,0:T(8,128)(2,1)S(1)} %get-tuple-element.13), channel_id=1, source_target_pairs={{0,32},{1,33},{2,34},{3,35},{4,0},{5,1},{6,2},{7,3},{8,40},{9,41},... | collective-permute-start | bytes 1179656 | tf_op jit(solution)/shard_map/ppermute | solution.py:229
  50.9 14.8 %collective-permute-start.3 = (bf16[3,32,2048]{2,1,0:T(8,128)(2,1)S(1)}, bf16[3,32,2048]{2,1,0:T(8,128)(2,1)S(1)}, u32[]{:S(2)}, u32[]{:S(2)}) collective-permute-start(bf16[3,32,2048]{2,1,0:T(8,128)(2,1)S(1)} %get-tuple-element.14), channel_id=1, source_target_pairs={{0,33},{1,32},{2,35},{3,34},{4,1},{5,0},{6,3},{7,2},{8,41},{9,40},... | collective-permute-start | bytes 1179656 | tf_op jit(solution)/shard_map/ppermute | solution.py:229
  54.9 17.3 %copy-start.8 = (bf16[3,32,2048]{2,1,0:T(8,128)(2,1)}, bf16[3,32,2048]{2,1,0:T(8,128)(2,1)S(1)}, u32[]{:S(2)}) copy-start(bf16[3,32,2048]{2,1,0:T(8,128)(2,1)S(1)} %collective-permute-done.refs_0_) | copy-start | bytes 1179652
  54.9 15.9 %collective-permute-start.4 = (bf16[3,32,2048]{2,1,0:T(8,128)(2,1)S(1)}, bf16[3,32,2048]{2,1,0:T(8,128)(2,1)S(1)}, u32[]{:S(2)}, u32[]{:S(2)}) collective-permute-start(bf16[3,32,2048]{2,1,0:T(8,128)(2,1)S(1)} %collective-permute-done.refs_0_), channel_id=1, source_target_pairs={{0,32},{32,0},{1,33},{33,1},{2,34},{34,2},{3,35},{35,3},{4,36},{36... | collective-permute-start | bytes 1179656 | tf_op jit(solution)/shard_map/ppermute | solution.py:232
  59.8 12.4 %copy-start.9 = (bf16[3,32,2048]{2,1,0:T(8,128)(2,1)}, bf16[3,32,2048]{2,1,0:T(8,128)(2,1)S(1)}, u32[]{:S(2)}) copy-start(bf16[3,32,2048]{2,1,0:T(8,128)(2,1)S(1)} %collective-permute-done.1.refs_1_) | copy-start | bytes 1179652
  59.8 11.0 %collective-permute-start.5 = (bf16[3,32,2048]{2,1,0:T(8,128)(2,1)S(1)}, bf16[3,32,2048]{2,1,0:T(8,128)(2,1)}, u32[]{:S(2)}, u32[]{:S(2)}) collective-permute-start(bf16[3,32,2048]{2,1,0:T(8,128)(2,1)S(1)} %collective-permute-done.1.refs_1_), channel_id=1, source_target_pairs={{0,32},{32,0},{1,33},{33,1},{2,34},{34,2},{3,35},{35,3},{4,36},{36... | collective-permute-start | bytes 1179656 | tf_op jit(solution)/shard_map/ppermute | solution.py:232
  61.7 10.5 %copy-start.10 = (bf16[3,32,2048]{2,1,0:T(8,128)(2,1)}, bf16[3,32,2048]{2,1,0:T(8,128)(2,1)S(1)}, u32[]{:S(2)}) copy-start(bf16[3,32,2048]{2,1,0:T(8,128)(2,1)S(1)} %collective-permute-done.2.refs_2_) | copy-start | bytes 1179652
  61.8 9.1 %collective-permute-start.6 = (bf16[3,32,2048]{2,1,0:T(8,128)(2,1)S(1)}, bf16[3,32,2048]{2,1,0:T(8,128)(2,1)}, u32[]{:S(2)}, u32[]{:S(2)}) collective-permute-start(bf16[3,32,2048]{2,1,0:T(8,128)(2,1)S(1)} %collective-permute-done.2.refs_2_), channel_id=1, source_target_pairs={{0,32},{32,0},{1,33},{33,1},{2,34},{34,2},{3,35},{35,3},{4,36},{36... | collective-permute-start | bytes 1179656 | tf_op jit(solution)/shard_map/ppermute | solution.py:232
  65.7 6.6 %copy-start.11 = (bf16[3,32,2048]{2,1,0:T(8,128)(2,1)}, bf16[3,32,2048]{2,1,0:T(8,128)(2,1)S(1)}, u32[]{:S(2)}) copy-start(bf16[3,32,2048]{2,1,0:T(8,128)(2,1)S(1)} %collective-permute-done.3.refs_3_) | copy-start | bytes 1179652
  65.7 6.6 %collective-permute-start.7 = (bf16[3,32,2048]{2,1,0:T(8,128)(2,1)S(1)}, bf16[3,32,2048]{2,1,0:T(8,128)(2,1)}, u32[]{:S(2)}, u32[]{:S(2)}) collective-permute-start(bf16[3,32,2048]{2,1,0:T(8,128)(2,1)S(1)} %collective-permute-done.3.refs_3_), channel_id=1, source_target_pairs={{0,32},{32,0},{1,33},{33,1},{2,34},{34,2},{3,35},{35,3},{4,36},{36... | collective-permute-start | bytes 1179656 | tf_op jit(solution)/shard_map/ppermute | solution.py:232
  70.8 1.5 %copy-start.12 = (bf16[3,32,2048]{2,1,0:T(8,128)(2,1)}, bf16[3,32,2048]{2,1,0:T(8,128)(2,1)S(1)}, u32[]{:S(2)}) copy-start(bf16[3,32,2048]{2,1,0:T(8,128)(2,1)S(1)} %collective-permute-done.4.refs_4_) | copy-start | bytes 1179652
  99.5 3.6 %copy-start.7 = (s32[16,4]{0,1:T(4,128)S(1)}, s32[16,4]{0,1:T(4,128)}, u32[]{:S(2)}) copy-start(s32[16,4]{0,1:T(4,128)} %param.12) | copy-start | bytes 772
  99.5 13.2 %all-to-all-start.3 = ((bf16[12,16,128]{2,1,0:T(8,128)(2,1)}), bf16[12,16,128]{2,1,0:T(8,128)(2,1)S(1)}, u32[]{:S(2)}, u32[]{:S(2)}) async-start(bf16[12,16,128]{2,1,0:T(8,128)(2,1)} %bitcast.5), calls=%async_computation.3 | async-start | bytes 98304 | tf_op jit(solution)/shard_map/all_to_all | solution.py:261
  103.1 0.7 copy-start.13
  (1 other events, 0.7 us)
where the time goes:
time: 116 us; the launch traced here: 114 us
  starting transfers between devices  56 us (48%)
  blocking collectives  23.3 us (20%)
  waiting for transfers between devices  22.9 us (20%)
  Pallas kernels  8.21 us (7%)
  local copies, waits for them, and re-layouts  2.79 us (2%)
    all_to_all x1, blocking collectives, per_device(): parts = lax.all_to_all(parts, ('y', 'x'), 0, 0, tiled=True)  23.3 us
    all_to_all x1, starting transfers between devices, per_device(): lax.all_to_all(packed.reshape(N_Z, LOCAL, LANES), 'z', 0, 0, tiled=True)  15.7 us
    ppermute x4, starting transfers between devices, per_device(): mine.append(lax.ppermute(piece, ('c', 'y', 'x'), pairs))  14.2 us
    ppermute x4, starting transfers between devices, per_device(): other.append(lax.ppermute(piece, 'c', [(0, 1), (1, 0)]))  12.8 us
    all_to_all x1, starting transfers between devices, per_device(): rows = lax.all_to_all(spread, ('y', 'x'), 0, 0, tiled=True)  9.67 us
    all_to_all x1, waiting for transfers between devices, per_device(): lax.all_to_all(packed.reshape(N_Z, LOCAL, LANES), 'z', 0, 0, tiled=True)  9.65 us
    all_to_all x1, waiting for transfers between devices, per_device(): lax.all_to_all(answers.reshape(N_Z, LOCAL, LANES), 'z', 0, 0, tiled=True)  8.62 us
    pallas_call x7, Pallas kernels, call(): pl.pallas_call(body, in_specs=ins, out_specs=[VMEM] * len(shapes), out_sh...  8.21 us
  transfers between devices with their start and end apart: 11, of which 5 were waited for; matrix products, arithmetic and copies ran while one was open for 0% of the time, Pallas kernels for 2%

commit v1 on v0

v1 whole, which is shorter than its diff:
```python
import jax
import jax.numpy as jnp
from jax import lax
from jax.experimental import pallas as pl
from jax.experimental.pallas import tpu as pltpu
from jax.sharding import Mesh, PartitionSpec as P

norm_eps = 1e-06
f32 = jnp.float32
bf16 = jnp.bfloat16

N_Z, N_C, N_Y, N_X = 12, 2, 8, 4
N_TP = N_Y * N_X
N_Q = 4
CAP = 3
TOK = 16
CAP = 3
TOK = 16
ROWS = N_Z * CAP
PADDED = 40
LANES = 128
HALF = 2048
UNITS = 32


def iota(shape, dim):
    return lax.broadcasted_iota(jnp.int32, shape, dim)


def dot(a, b, dims, precision=None):
    return lax.dot_general(a, b, (dims, ((), ())), preferred_element_type=f32, precision=precision)


def copies_body(hidden_ref, out_ref):
    for j in range(N_TP):
        out_ref[j] = hidden_ref[...]


def slot_of(shape, dim):
    row = iota(shape, dim)
    block = jnp.floor((row.astype(f32) + 0.5) * (1.0 / CAP)).astype(jnp.int32)
    return block, (row - CAP * block).astype(f32)


def tables_body(place_ref, across_ref, routes_ref, weights_ref, select_ref, combine_ref):
    place = place_ref[0]
    block, wanted = slot_of((PADDED, TOK), 0)
    named = jnp.zeros((PADDED, TOK), f32)
    for k in range(4):
        named = named + jnp.where(across_ref[k : k + 1, :] == N_Q * block + place, 1.0, 0.0)
    earlier = jnp.where(iota((TOK, TOK), 0) < iota((TOK, TOK), 1), 1.0, 0.0).astype(bf16)
    rank = dot(named.astype(bf16), earlier, ((1,), (0,)))
    select_ref[...] = jnp.where(rank == wanted, named, 0.0).astype(bf16)
    block, wanted = slot_of((TOK, PADDED), 1)
    named = jnp.zeros((TOK, PADDED), f32)
    total = jnp.zeros((TOK, PADDED), f32)
    for k in range(4):
        hit = routes_ref[:, k : k + 1] == N_Q * block + place
        named = named + jnp.where(hit, 1.0, 0.0)
        total = total + jnp.where(hit, weights_ref[:, k : k + 1], 0.0)
    earlier = jnp.where(iota((TOK, TOK), 1) < iota((TOK, TOK), 0), 1.0, 0.0).astype(bf16)
    rank = dot(earlier, named.astype(bf16), ((1,), (0,)))
    combine_ref[...] = jnp.where(rank == wanted, total, 0.0)


def norm_body(rows_ref, gain_ref, select_ref, own_ref, out_ref, flat):
    squares = jnp.zeros((TOK, LANES), f32)
    for s in range(N_TP):
        v = rows_ref[s].astype(f32)
        squares = squares + v * v
    inv = lax.rsqrt(jnp.sum(squares, axis=1, keepdims=True) * (1.0 / (N_TP * LANES)) + norm_eps)
    select = select_ref[...]
    for s in range(N_TP):
        piece = (rows_ref[s].astype(f32) * inv * gain_ref[s]).astype(bf16)
        own_ref[:, s * LANES : (s + 1) * LANES] = piece
        flat[pl.ds(s, ROWS, stride=N_TP), :] = dot(select, piece, ((1,), (0,)))[0:ROWS]
    out_ref[...] = flat[...].astype(bf16)


def weights_body(pos_ref, gate_ref, up_ref, down_ref, o0, o1, o2, o3, sems):
    copies = []
    for m, out in enumerate((o0, o1, o2, o3)):
        v = pos_ref[m]
        for w, ref in enumerate((gate_ref, up_ref, down_ref)):
            copy = pltpu.make_async_copy(
                ref.at[v % 2, :, pl.ds((v // 2) * HALF, HALF)], out.at[w], sems.at[m, w]
            )
            copy.start()
            copies.append(copy)
    for copy in copies:
        copy.wait()


def silu(v):
    return v / (1.0 + jnp.exp(-v))


def shared_body(own_ref, gate_ref, up_ref, down_ref, out_ref):
    own = own_ref[...]
    nt = ((1,), (1,))
    inner = (silu(dot(own, gate_ref[...], nt)) * dot(own, up_ref[...], nt)).astype(bf16)
    out_ref[...] = dot(inner, down_ref[...], ((1,), (0,)))


def experts_body(core_ref, rows_ref, *refs):
    given, (out_ref, flat, pieces, held, sems) = refs[:8], refs[8:]
    copies = [pltpu.make_async_copy(given[i], held.at[i], sems.at[i]) for i in range(8)]
    for copy in copies:
        copy.start()
    core = core_ref[0]
    flat[...] = rows_ref[...].astype(f32)
    for s in range(N_TP):
        pieces[s] = flat[pl.ds(s, ROWS, stride=N_TP), :].astype(bf16)

    def wide(first):
        return jnp.concatenate([pieces[first + s] for s in range(N_TP // 2)], axis=1)

    x_mine = wide(core * (N_TP // 2))
    x_other = wide((1 - core) * (N_TP // 2))
    mine = (0, 1, 2, 3)
    other = (6, 7, 4, 5)
    nt, nn = ((1,), (1,)), ((1,), (0,))
    for copy in copies:
        copy.wait()

    def project(w):
        w_mine = jnp.concatenate([held[i, w] for i in mine], axis=0)
        w_other = jnp.concatenate([held[i, w] for i in other], axis=0)
        return dot(x_mine, w_mine, nt) + dot(x_other, w_other, nt)

    inner = (silu(project(0)) * project(1)).astype(bf16)
    for side, slots in ((core, mine), (1 - core, other)):
        w = jnp.concatenate([held[i, 2] for i in slots], axis=0)
        part = dot(inner, w, nn)
        for s in range(N_TP // 2):
            flat[pl.ds(side * (N_TP // 2) + s, ROWS, stride=N_TP), :] = part[
                :, s * LANES : (s + 1) * LANES
            ]
    out_ref[...] = flat[...].astype(bf16)


def combine_body(rows_ref, combine_ref, shared_ref, out_ref, flat):
    flat[...] = rows_ref[...].astype(f32)
    combine = combine_ref[:, 0:ROWS]
    for s in range(N_TP):
        piece = flat[pl.ds(s, ROWS, stride=N_TP), :]
        total = dot(combine, piece, ((1,), (0,)), lax.Precision.HIGHEST)
        out_ref[s] = (total + shared_ref[:, s * LANES : (s + 1) * LANES]).astype(bf16)


def sum_body(parts_ref, out_ref):
    total = jnp.zeros((TOK, LANES), f32)
    for s in range(N_TP):
        total = total + parts_ref[s].astype(f32)
    out_ref[...] = total.astype(bf16)


VMEM = pl.BlockSpec(memory_space=pltpu.VMEM)
SMEM = pl.BlockSpec(memory_space=pltpu.SMEM)
ANY = pl.BlockSpec(memory_space=pl.ANY)


def call(body, ins, outs, *args, scratch=(), limit=4):
    single = not isinstance(outs, list)
    shapes = [outs] if single else outs
    spaces = {id(VMEM): pltpu.VMEM, id(ANY): pltpu.HBM}
    args = [
        pltpu.with_memory_space_constraint(arg, spaces[id(spec)]) if id(spec) in spaces else arg
        for spec, arg in zip(ins, args, strict=True)
    ]
    got = pl.pallas_call(
        body,
        in_specs=ins,
        out_specs=[VMEM] * len(shapes),
        out_shape=shapes,
        scratch_shapes=list(scratch),
        compiler_params=pltpu.CompilerParams(vmem_limit_bytes=limit << 20),
    )(*args)
    return got[0] if single else got


def shape(dims, dtype=bf16):
    return pltpu.VMEM(dims, dtype)


def per_device(
    hidden,
    norm_gain,
    routes,
    route_weights,
    gate_weight,
    up_weight,
    down_weight,
    shared_gate,
    shared_up,
    shared_down,
):
    core, y, x = lax.axis_index("c"), lax.axis_index("y"), lax.axis_index("x")
    place = 2 * (y % 2) + x % 2
    copies = call(copies_body, [VMEM], shape((N_TP, TOK, LANES)), hidden)
    tokens = lax.all_to_all(copies, ("y", "x"), 0, 0, tiled=True)
    select, combine = call(
        tables_body,
        [SMEM] + [VMEM] * 3,
        [shape((PADDED, TOK)), shape((TOK, PADDED), f32)],
        place.reshape(1).astype(jnp.int32),
        routes.T,
        routes,
        route_weights,
    )
    order = jnp.bitwise_xor(place, jnp.arange(4, dtype=jnp.int32))
    pieces = call(
        weights_body,
        [SMEM, ANY, ANY, ANY],
        [shape((3, UNITS, HALF))] * 4,
        order,
        gate_weight,
        up_weight,
        down_weight,
        scratch=[pltpu.SemaphoreType.DMA((4, 3))],
    )
    mine = []
    for m, piece in enumerate(pieces):
        pairs = []
        for c in range(N_C):
            for j in range(N_TP):
                sy, sx = j // N_X, j % N_X
                v = (2 * (sy % 2) + sx % 2) ^ m
                target = (v // 2) * N_TP + (sy - sy % 2 + c) * N_X + (sx - sx % 2 + v % 2)
                pairs.append((c * N_TP + j, target))
        mine.append(lax.ppermute(piece, ("c", "y", "x"), pairs))
    other = []
    for piece in mine:
        other.append(lax.ppermute(piece, "c", [(0, 1), (1, 0)]))
    flat = pltpu.VMEM((ROWS * N_TP, LANES), f32)
    own, packed = call(
        norm_body,
        [VMEM] * 3,
        [shape((TOK, N_TP * LANES)), shape((ROWS * N_TP, LANES))],
        tokens,
        norm_gain.reshape(N_TP, 1, LANES),
        select,
        scratch=[flat],
    )
    arrived = lax.all_to_all(packed.reshape(N_Z, CAP * N_TP, LANES), "z", 0, 0, tiled=True)
    shared = call(
        shared_body,
        [VMEM] * 4,
        shape((TOK, N_TP * LANES), f32),
        own,
        shared_gate,
        shared_up,
        shared_down,
    )
    parts = call(
        experts_body,
        [SMEM, VMEM] + [ANY] * 8,
        shape((ROWS * N_TP, LANES)),
        core.reshape(1).astype(jnp.int32),
        arrived.reshape(ROWS * N_TP, LANES),
        *mine,
        *other,
        scratch=[
            flat,
            pltpu.VMEM((N_TP, ROWS, LANES), bf16),
            pltpu.VMEM((8, 3, UNITS, HALF), bf16),
            pltpu.SemaphoreType.DMA((8,)),
        ],
        limit=24,
    )
    returned = lax.all_to_all(parts.reshape(N_Z, CAP * N_TP, LANES), "z", 0, 0, tiled=True)
    mixed = call(
        combine_body,
        [VMEM] * 3,
        shape((N_TP, TOK, LANES)),
        returned.reshape(ROWS * N_TP, LANES),
        combine,
        shared,
        scratch=[flat],
    )
    mixed = lax.all_to_all(mixed, ("y", "x"), 0, 0, tiled=True)
    return call(sum_body, [VMEM], shape((TOK, LANES)), mixed)


def solution(mesh):
    fine = Mesh(mesh.devices.reshape(N_Z, N_C, N_Y, N_X), ("z", "c", "y", "x"))
    ep, tp = ("z", "c"), ("y", "x")
    in_specs = (
        P(ep, tp),
        P(),
        P(ep, None),
        P(ep, None),
        P(ep, tp, None),
        P(ep, tp, None),
        P(ep, tp, None),
        P(tp, None),
        P(tp, None),
        P(tp, None),
    )

    return jax.shard_map(
        per_device, mesh=fine, in_specs=in_specs, out_specs=P(ep, tp), check_vma=False
    )
```

time: 116 us -> 114 us (0.983)
  the two profiles are of different devices: /device:TPU:1 before, /device:TPU:64 now
where the time goes in v1:
time: 114 us; the launch traced here: 113 us
  starting transfers between devices  54.7 us (48%)
  waiting for transfers between devices  31.3 us (27%)
  blocking collectives  13.9 us (12%)
  Pallas kernels  9.67 us (8%)
  local copies, waits for them, and re-layouts  3.44 us (3%)
    all_to_all x1, waiting for transfers between devices, per_device(): lax.all_to_all(parts.reshape(N_Z, CAP * N_TP, LANES), 'z', 0, 0, tiled=True)  16.8 us
    all_to_all x1, starting transfers between devices, per_device(): lax.all_to_all(packed.reshape(N_Z, CAP * N_TP, LANES), 'z', 0, 0, tiled=T...  14.8 us
    all_to_all x1, blocking collectives, per_device(): mixed = lax.all_to_all(mixed, ('y', 'x'), 0, 0, tiled=True)  13.9 us
    ppermute x4, starting transfers between devices, per_device(): other.append(lax.ppermute(piece, 'c', [(0, 1), (1, 0)]))  10.3 us
    all_to_all x1, starting transfers between devices, per_device(): tokens = lax.all_to_all(copies, ('y', 'x'), 0, 0, tiled=True)  9.95 us
    ppermute x4, starting transfers between devices, per_device(): mine.append(lax.ppermute(piece, ('c', 'y', 'x'), pairs))  9.83 us
    all_to_all x1, starting transfers between devices, per_device(): lax.all_to_all(parts.reshape(N_Z, CAP * N_TP, LANES), 'z', 0, 0, tiled=True)  9.76 us
    pallas_call x8, Pallas kernels, call(): pl.pallas_call(body, in_specs=ins, out_specs=[VMEM] * len(shapes), out_sh...  9.67 us
  transfers between devices with their start and end apart: 11, of which 6 were waited for; matrix products, arithmetic and copies ran while one was open for 0% of the time, Pallas kernels for 2%

profile of v1, /device:TPU:64, one launch (start us, length us, event | category | flops | bytes accessed | tf_op | source)
XLA Modules:
  0.0 113.2 jit_solution(13502083987175532285)
XLA Ops:
  0.0 0.7 copy-done.5
  1.4 10.0 %all-to-all-start = ((bf16[32,16,128]{2,1,0:T(8,128)(2,1)}), bf16[32,16,128]{2,1,0:T(8,128)(2,1)S(1)}, u32[]{:S(2)}, u32[]{:S(2)}) async-start(bf16[32,16,128]{2,1,0:T(8,128)(2,1)} %shard_map.100), calls=%async_computation | async-start | bytes 262144 | tf_op jit(solution)/shard_map/all_to_all | solution.py:201
  11.3 0.7 copy-done.4
  13.0 8.8 %all-to-all-done.rows_ref = bf16[32,16,128]{2,1,0:T(8,128)(2,1)S(1)} async-done(((bf16[32,16,128]{2,1,0:T(8,128)(2,1)}), bf16[32,16,128]{2,1,0:T(8,128)(2,1)S(1)}, u32[]{:S(2)}, u32[]{:S(2)}) %all-to-all-start) | async-done | bytes 131104 | tf_op jit(solution)/shard_map/all_to_all | solution.py:201
  21.8 1.4 %shard_map.102 = (bf16[16,4096]{1,0:T(8,128)(2,1)S(1)}, bf16[1152,128]{1,0:T(8,128)(2,1)}) custom-call(bf16[32,16,128]{2,1,0:T(8,128)(2,1)S(1)} %all-to-all-done.rows_ref, f32[32,1,128]{2,1,0:T(1,128)S(1)} %bitcast.10, bf16[40,16]{1,0:T(8,128)(2,1)S(1)} %get-tuple-element.13.select_ref), custom_call_target="tpu_custom_call" | custom-call | tf_op jit(solution)/shard_map/pallas_call | solution.py:171
  23.2 14.8 %all-to-all-start.1 = ((bf16[12,96,128]{2,1,0:T(8,128)(2,1)}), bf16[12,96,128]{2,1,0:T(8,128)(2,1)S(1)}, u32[]{:S(2)}, u32[]{:S(2)}) async-start(bf16[12,96,128]{2,1,0:T(8,128)(2,1)} %bitcast.4), calls=%async_computation.1 | async-start | bytes 589824 | tf_op jit(solution)/shard_map/all_to_all | solution.py:245
  38.0 2.1 %shard_map.103 = (bf16[3,32,2048]{2,1,0:T(8,128)(2,1)S(1)}, bf16[3,32,2048]{2,1,0:T(8,128)(2,1)S(1)}, bf16[3,32,2048]{2,1,0:T(8,128)(2,1)S(1)}, bf16[3,32,2048]{2,1,0:T(8,128)(2,1)S(1)}) custom-call(s32[4]{0:T(128)S(1)} %iota_xor_fusion.pos_ref, bf16[2,32,4096]{2,1,0:T(8,128)(2,1)} %gate_ref.2, bf16[2,32,4096]{2,1,0:T(8,128)(2,1)} %up_ref.2, ...), custom_call_target="tpu_custom_call" | custom-call | tf_op jit(solution)/shard_map/pallas_call | solution.py:171
  40.1 0.7 collective-permute-start
  40.8 2.1 %collective-permute-start.1 = (bf16[3,32,2048]{2,1,0:T(8,128)(2,1)S(1)}, bf16[3,32,2048]{2,1,0:T(8,128)(2,1)S(1)}, u32[]{:S(2)}, u32[]{:S(2)}) collective-permute-start(bf16[3,32,2048]{2,1,0:T(8,128)(2,1)S(1)} %get-tuple-element.16), channel_id=1, source_target_pairs={{0,1},{1,0},{2,3},{3,2},{4,33},{5,32},{6,35},{7,34},{8,9},{9,8},{1... | collective-permute-start | bytes 1179656 | tf_op jit(solution)/shard_map/ppermute | solution.py:231
  42.9 4.1 %collective-permute-start.2 = (bf16[3,32,2048]{2,1,0:T(8,128)(2,1)S(1)}, bf16[3,32,2048]{2,1,0:T(8,128)(2,1)S(1)}, u32[]{:S(2)}, u32[]{:S(2)}) collective-permute-start(bf16[3,32,2048]{2,1,0:T(8,128)(2,1)S(1)} %get-tuple-element.17), channel_id=1, source_target_pairs={{0,32},{1,33},{2,34},{3,35},{4,0},{5,1},{6,2},{7,3},{8,40},{9,41},... | collective-permute-start | bytes 1179656 | tf_op jit(solution)/shard_map/ppermute | solution.py:231
  46.9 3.0 %collective-permute-start.3 = (bf16[3,32,2048]{2,1,0:T(8,128)(2,1)S(1)}, bf16[3,32,2048]{2,1,0:T(8,128)(2,1)S(1)}, u32[]{:S(2)}, u32[]{:S(2)}) collective-permute-start(bf16[3,32,2048]{2,1,0:T(8,128)(2,1)S(1)} %get-tuple-element.18), channel_id=1, source_target_pairs={{0,33},{1,32},{2,35},{3,34},{4,1},{5,0},{6,3},{7,2},{8,41},{9,40},... | collective-permute-start | bytes 1179656 | tf_op jit(solution)/shard_map/ppermute | solution.py:231
  50.0 3.6 %collective-permute-start.4 = (bf16[3,32,2048]{2,1,0:T(8,128)(2,1)S(1)}, bf16[3,32,2048]{2,1,0:T(8,128)(2,1)S(1)}, u32[]{:S(2)}, u32[]{:S(2)}) collective-permute-start(bf16[3,32,2048]{2,1,0:T(8,128)(2,1)S(1)} %collective-permute-done.refs_0_), channel_id=1, source_target_pairs={{0,32},{32,0},{1,33},{33,1},{2,34},{34,2},{3,35},{35,3},{4,36},{36... | collective-permute-start | bytes 1179656 | tf_op jit(solution)/shard_map/ppermute | solution.py:234
  53.5 1.1 collective-permute-done.1.refs_1_
  54.7 1.9 %collective-permute-start.5 = (bf16[3,32,2048]{2,1,0:T(8,128)(2,1)S(1)}, bf16[3,32,2048]{2,1,0:T(8,128)(2,1)}, u32[]{:S(2)}, u32[]{:S(2)}) collective-permute-start(bf16[3,32,2048]{2,1,0:T(8,128)(2,1)S(1)} %collective-permute-done.1.refs_1_), channel_id=1, source_target_pairs={{0,32},{32,0},{1,33},{33,1},{2,34},{34,2},{3,35},{35,3},{4,36},{36... | collective-permute-start | bytes 1179656 | tf_op jit(solution)/shard_map/ppermute | solution.py:234
  57.2 1.9 %collective-permute-start.6 = (bf16[3,32,2048]{2,1,0:T(8,128)(2,1)S(1)}, bf16[3,32,2048]{2,1,0:T(8,128)(2,1)S(1)}, u32[]{:S(2)}, u32[]{:S(2)}) collective-permute-start(bf16[3,32,2048]{2,1,0:T(8,128)(2,1)S(1)} %collective-permute-done.2.refs_2_), channel_id=1, source_target_pairs={{0,32},{32,0},{1,33},{33,1},{2,34},{34,2},{3,35},{35,3},{4,36},{36... | collective-permute-start | bytes 1179656 | tf_op jit(solution)/shard_map/ppermute | solution.py:234
  59.1 2.7 %collective-permute-done.3.refs_3_ = bf16[3,32,2048]{2,1,0:T(8,128)(2,1)S(1)} collective-permute-done((bf16[3,32,2048]{2,1,0:T(8,128)(2,1)S(1)}, bf16[3,32,2048]{2,1,0:T(8,128)(2,1)S(1)}, u32[]{:S(2)}, u32[]{:S(2)}) %collective-permute-start.3) | collective-permute-done | bytes 393248 | tf_op jit(solution)/shard_map/ppermute | solution.py:231
  61.8 3.0 %collective-permute-start.7 = (bf16[3,32,2048]{2,1,0:T(8,128)(2,1)S(1)}, bf16[3,32,2048]{2,1,0:T(8,128)(2,1)S(1)}, u32[]{:S(2)}, u32[]{:S(2)}) collective-permute-start(bf16[3,32,2048]{2,1,0:T(8,128)(2,1)S(1)} %collective-permute-done.3.refs_3_), channel_id=1, source_target_pairs={{0,32},{32,0},{1,33},{33,1},{2,34},{34,2},{3,35},{35,3},{4,36},{36... | collective-permute-start | bytes 1179656 | tf_op jit(solution)/shard_map/ppermute | solution.py:234
  64.9 1.3 %collective-permute-done.7.refs_7_ = bf16[3,32,2048]{2,1,0:T(8,128)(2,1)S(1)} collective-permute-done((bf16[3,32,2048]{2,1,0:T(8,128)(2,1)S(1)}, bf16[3,32,2048]{2,1,0:T(8,128)(2,1)S(1)}, u32[]{:S(2)}, u32[]{:S(2)}) %collective-permute-start.7) | collective-permute-done | bytes 393248 | tf_op jit(solution)/shard_map/ppermute | solution.py:234
  66.2 0.7 copy-done.12
  66.9 4.0 %shard_map.104 = bf16[1152,128]{1,0:T(8,128)(2,1)} custom-call(s32[1]{0:T(128)} %bitcast.core_ref, bf16[1152,128]{1,0:T(8,128)(2,1)S(1)} %bitcast.9, bf16[3,32,2048]{2,1,0:T(8,128)(2,1)} %copy-done.6, bf16[3,32,2048]{2,1,0:T(8,128)(2,1)} %copy-done.7, bf16[3,32,2048]{2,1,0:T(8,128)(2,1)} %copy-done.8, bf16[3,32,2048]{2,1,0:T(8,128)(2,1)} %copy-done.9, ...), custom_call_target="tpu_custom_call" | custom-call | tf_op jit(solution)/shard_map/pallas_call | solution.py:171
  70.9 9.8 %all-to-all-start.2 = ((bf16[12,96,128]{2,1,0:T(8,128)(2,1)}), bf16[12,96,128]{2,1,0:T(8,128)(2,1)S(1)}, u32[]{:S(2)}, u32[]{:S(2)}) async-start(bf16[12,96,128]{2,1,0:T(8,128)(2,1)} %bitcast.6), calls=%async_computation.2 | async-start | bytes 589824 | tf_op jit(solution)/shard_map/all_to_all | solution.py:271
  81.1 16.8 %all-to-all-done.2 = bf16[12,96,128]{2,1,0:T(8,128)(2,1)S(1)} async-done(((bf16[12,96,128]{2,1,0:T(8,128)(2,1)}), bf16[12,96,128]{2,1,0:T(8,128)(2,1)S(1)}, u32[]{:S(2)}, u32[]{:S(2)}) %all-to-all-start.2) | async-done | bytes 294944 | tf_op jit(solution)/shard_map/all_to_all | solution.py:271
  97.9 0.8 shard_map.106
  98.7 13.9 %all_to_all.20.parts_ref = bf16[32,16,128]{2,1,0:T(8,128)(2,1)S(1)} all-to-all(bf16[32,16,128]{2,1,0:T(8,128)(2,1)S(1)} %shard_map.106), channel_id=1, replica_groups=mesh['z'=12,'c'=2,'y'=8,'x'=4] {'y','x'}, dimensions={0} | all-to-all | bytes 262144 | tf_op jit(solution)/shard_map/all_to_all | solution.py:281
  (39 shorter events, 3.4 us)
Async XLA Ops:
  0.0 0.7 copy-start.5
  1.4 20.4 %all-to-all-start = ((bf16[32,16,128]{2,1,0:T(8,128)(2,1)}), bf16[32,16,128]{2,1,0:T(8,128)(2,1)S(1)}, u32[]{:S(2)}, u32[]{:S(2)}) async-start(bf16[32,16,128]{2,1,0:T(8,128)(2,1)} %shard_map.100), calls=%async_computation | async-start | bytes 262144 | tf_op jit(solution)/shard_map/all_to_all | solution.py:201
  11.3 0.7 copy-start.4
  12.8 9.0 %copy-start.3 = (f32[4096]{0:T(1024)S(1)}, f32[4096]{0:T(1024)}, u32[]{:S(2)}) copy-start(f32[4096]{0:T(1024)} %param.11) | copy-start | bytes 49156
  23.2 43.0 %all-to-all-start.1 = ((bf16[12,96,128]{2,1,0:T(8,128)(2,1)}), bf16[12,96,128]{2,1,0:T(8,128)(2,1)S(1)}, u32[]{:S(2)}, u32[]{:S(2)}) async-start(bf16[12,96,128]{2,1,0:T(8,128)(2,1)} %bitcast.4), calls=%async_computation.1 | async-start | bytes 589824 | tf_op jit(solution)/shard_map/all_to_all | solution.py:245
  40.1 9.9 %collective-permute-start = (bf16[3,32,2048]{2,1,0:T(8,128)(2,1)S(1)}, bf16[3,32,2048]{2,1,0:T(8,128)(2,1)S(1)}, u32[]{:S(2)}, u32[]{:S(2)}) collective-permute-start(bf16[3,32,2048]{2,1,0:T(8,128)(2,1)S(1)} %get-tuple-element.15), channel_id=1, source_target_pairs={{0,0},{1,1},{2,2},{3,3},{4,32},{5,33},{6,34},{7,35},{8,8},{9,9},{1... | collective-permute-start | bytes 1179656 | tf_op jit(solution)/shard_map/ppermute | solution.py:231
  40.8 13.9 %collective-permute-start.1 = (bf16[3,32,2048]{2,1,0:T(8,128)(2,1)S(1)}, bf16[3,32,2048]{2,1,0:T(8,128)(2,1)S(1)}, u32[]{:S(2)}, u32[]{:S(2)}) collective-permute-start(bf16[3,32,2048]{2,1,0:T(8,128)(2,1)S(1)} %get-tuple-element.16), channel_id=1, source_target_pairs={{0,1},{1,0},{2,3},{3,2},{4,33},{5,32},{6,35},{7,34},{8,9},{9,8},{1... | collective-permute-start | bytes 1179656 | tf_op jit(solution)/shard_map/ppermute | solution.py:231
  42.9 14.3 %collective-permute-start.2 = (bf16[3,32,2048]{2,1,0:T(8,128)(2,1)S(1)}, bf16[3,32,2048]{2,1,0:T(8,128)(2,1)S(1)}, u32[]{:S(2)}, u32[]{:S(2)}) collective-permute-start(bf16[3,32,2048]{2,1,0:T(8,128)(2,1)S(1)} %get-tuple-element.17), channel_id=1, source_target_pairs={{0,32},{1,33},{2,34},{3,35},{4,0},{5,1},{6,2},{7,3},{8,40},{9,41},... | collective-permute-start | bytes 1179656 | tf_op jit(solution)/shard_map/ppermute | solution.py:231
  46.9 14.9 %collective-permute-start.3 = (bf16[3,32,2048]{2,1,0:T(8,128)(2,1)S(1)}, bf16[3,32,2048]{2,1,0:T(8,128)(2,1)S(1)}, u32[]{:S(2)}, u32[]{:S(2)}) collective-permute-start(bf16[3,32,2048]{2,1,0:T(8,128)(2,1)S(1)} %get-tuple-element.18), channel_id=1, source_target_pairs={{0,33},{1,32},{2,35},{3,34},{4,1},{5,0},{6,3},{7,2},{8,41},{9,40},... | collective-permute-start | bytes 1179656 | tf_op jit(solution)/shard_map/ppermute | solution.py:231
  49.9 16.2 %copy-start.6 = (bf16[3,32,2048]{2,1,0:T(8,128)(2,1)}, bf16[3,32,2048]{2,1,0:T(8,128)(2,1)S(1)}, u32[]{:S(2)}) copy-start(bf16[3,32,2048]{2,1,0:T(8,128)(2,1)S(1)} %collective-permute-done.refs_0_) | copy-start | bytes 1179652
  50.0 14.9 %collective-permute-start.4 = (bf16[3,32,2048]{2,1,0:T(8,128)(2,1)S(1)}, bf16[3,32,2048]{2,1,0:T(8,128)(2,1)S(1)}, u32[]{:S(2)}, u32[]{:S(2)}) collective-permute-start(bf16[3,32,2048]{2,1,0:T(8,128)(2,1)S(1)} %collective-permute-done.refs_0_), channel_id=1, source_target_pairs={{0,32},{32,0},{1,33},{33,1},{2,34},{34,2},{3,35},{35,3},{4,36},{36... | collective-permute-start | bytes 1179656 | tf_op jit(solution)/shard_map/ppermute | solution.py:234
  54.7 11.5 %copy-start.7 = (bf16[3,32,2048]{2,1,0:T(8,128)(2,1)}, bf16[3,32,2048]{2,1,0:T(8,128)(2,1)S(1)}, u32[]{:S(2)}) copy-start(bf16[3,32,2048]{2,1,0:T(8,128)(2,1)S(1)} %collective-permute-done.1.refs_1_) | copy-start | bytes 1179652
  54.7 10.2 %collective-permute-start.5 = (bf16[3,32,2048]{2,1,0:T(8,128)(2,1)S(1)}, bf16[3,32,2048]{2,1,0:T(8,128)(2,1)}, u32[]{:S(2)}, u32[]{:S(2)}) collective-permute-start(bf16[3,32,2048]{2,1,0:T(8,128)(2,1)S(1)} %collective-permute-done.1.refs_1_), channel_id=1, source_target_pairs={{0,32},{32,0},{1,33},{33,1},{2,34},{34,2},{3,35},{35,3},{4,36},{36... | collective-permute-start | bytes 1179656 | tf_op jit(solution)/shard_map/ppermute | solution.py:234
  57.2 9.0 %copy-start.8 = (bf16[3,32,2048]{2,1,0:T(8,128)(2,1)}, bf16[3,32,2048]{2,1,0:T(8,128)(2,1)S(1)}, u32[]{:S(2)}) copy-start(bf16[3,32,2048]{2,1,0:T(8,128)(2,1)S(1)} %collective-permute-done.2.refs_2_) | copy-start | bytes 1179652
  57.2 7.7 %collective-permute-start.6 = (bf16[3,32,2048]{2,1,0:T(8,128)(2,1)S(1)}, bf16[3,32,2048]{2,1,0:T(8,128)(2,1)S(1)}, u32[]{:S(2)}, u32[]{:S(2)}) collective-permute-start(bf16[3,32,2048]{2,1,0:T(8,128)(2,1)S(1)} %collective-permute-done.2.refs_2_), channel_id=1, source_target_pairs={{0,32},{32,0},{1,33},{33,1},{2,34},{34,2},{3,35},{35,3},{4,36},{36... | collective-permute-start | bytes 1179656 | tf_op jit(solution)/shard_map/ppermute | solution.py:234
  61.8 4.3 %copy-start.9 = (bf16[3,32,2048]{2,1,0:T(8,128)(2,1)}, bf16[3,32,2048]{2,1,0:T(8,128)(2,1)S(1)}, u32[]{:S(2)}) copy-start(bf16[3,32,2048]{2,1,0:T(8,128)(2,1)S(1)} %collective-permute-done.3.refs_3_) | copy-start | bytes 1179652
  61.8 4.3 %collective-permute-start.7 = (bf16[3,32,2048]{2,1,0:T(8,128)(2,1)S(1)}, bf16[3,32,2048]{2,1,0:T(8,128)(2,1)S(1)}, u32[]{:S(2)}, u32[]{:S(2)}) collective-permute-start(bf16[3,32,2048]{2,1,0:T(8,128)(2,1)S(1)} %collective-permute-done.3.refs_3_), channel_id=1, source_target_pairs={{0,32},{32,0},{1,33},{33,1},{2,34},{34,2},{3,35},{35,3},{4,36},{36... | collective-permute-start | bytes 1179656 | tf_op jit(solution)/shard_map/ppermute | solution.py:234
  64.8 1.4 %copy-start.10 = (bf16[3,32,2048]{2,1,0:T(8,128)(2,1)}, bf16[3,32,2048]{2,1,0:T(8,128)(2,1)S(1)}, u32[]{:S(2)}) copy-start(bf16[3,32,2048]{2,1,0:T(8,128)(2,1)S(1)} %collective-permute-done.4.refs_4_) | copy-start | bytes 1179652
  64.9 1.3 %copy-start.11 = (bf16[3,32,2048]{2,1,0:T(8,128)(2,1)}, bf16[3,32,2048]{2,1,0:T(8,128)(2,1)S(1)}, u32[]{:S(2)}) copy-start(bf16[3,32,2048]{2,1,0:T(8,128)(2,1)S(1)} %collective-permute-done.6.refs_6_) | copy-start | bytes 1179652
  66.1 0.7 copy-start.12
  66.9 13.8 %copy-start.2 = (bf16[32,4096]{1,0:T(8,128)(2,1)S(1)}, bf16[32,4096]{1,0:T(8,128)(2,1)}, u32[]{:S(2)}) copy-start(bf16[32,4096]{1,0:T(8,128)(2,1)} %down_ref.3) | copy-start | bytes 786436
  70.9 9.8 %copy-start = (bf16[32,4096]{1,0:T(8,128)(2,1)S(1)}, bf16[32,4096]{1,0:T(8,128)(2,1)}, u32[]{:S(2)}) copy-start(bf16[32,4096]{1,0:T(8,128)(2,1)} %gate_ref.3) | copy-start | bytes 786436
  70.9 9.8 %copy-start.1 = (bf16[32,4096]{1,0:T(8,128)(2,1)S(1)}, bf16[32,4096]{1,0:T(8,128)(2,1)}, u32[]{:S(2)}) copy-start(bf16[32,4096]{1,0:T(8,128)(2,1)} %up_ref.3) | copy-start | bytes 786436
  70.9 27.0 %all-to-all-start.2 = ((bf16[12,96,128]{2,1,0:T(8,128)(2,1)}), bf16[12,96,128]{2,1,0:T(8,128)(2,1)S(1)}, u32[]{:S(2)}, u32[]{:S(2)}) async-start(bf16[12,96,128]{2,1,0:T(8,128)(2,1)} %bitcast.6), calls=%async_computation.2 | async-start | bytes 589824 | tf_op jit(solution)/shard_map/all_to_all | solution.py:271
  (1 other events, 0.7 us)

commit v2 on v1

--- a/solution.py
+++ b/solution.py
@@ -19,7 +19,6 @@
 ROWS = N_Z * CAP
 PADDED = 40
 LANES = 128
-HALF = 2048
 UNITS = 32
 
 
@@ -77,16 +76,13 @@
     out_ref[...] = flat[...].astype(bf16)
 
 
-def weights_body(pos_ref, gate_ref, up_ref, down_ref, o0, o1, o2, o3, sems):
+def weights_body(first_ref, gate_ref, up_ref, down_ref, o0, o1, sems):
     copies = []
-    for m, out in enumerate((o0, o1, o2, o3)):
-        v = pos_ref[m]
+    for m, out in enumerate((o0, o1)):
+        expert = (first_ref[0] + m) % 2
         for w, ref in enumerate((gate_ref, up_ref, down_ref)):
-            copy = pltpu.make_async_copy(
-                ref.at[v % 2, :, pl.ds((v // 2) * HALF, HALF)], out.at[w], sems.at[m, w]
-            )
-            copy.start()
-            copies.append(copy)
+            copies.append(pltpu.make_async_copy(ref.at[expert], out.at[w], sems.at[m, w]))
+            copies[-1].start()
     for copy in copies:
         copy.wait()
 
@@ -102,40 +98,25 @@
     out_ref[...] = dot(inner, down_ref[...], ((1,), (0,)))
 
 
-def experts_body(core_ref, rows_ref, *refs):
-    given, (out_ref, flat, pieces, held, sems) = refs[:8], refs[8:]
-    copies = [pltpu.make_async_copy(given[i], held.at[i], sems.at[i]) for i in range(8)]
+def experts_body(rows_ref, g0, g1, g2, g3, out_ref, flat, held, sems):
+    copies = [
+        pltpu.make_async_copy(ref, held.at[:, pl.ds(i * UNITS, UNITS)], sems.at[i])
+        for i, ref in enumerate((g0, g1, g2, g3))
+    ]
     for copy in copies:
         copy.start()
-    core = core_ref[0]
     flat[...] = rows_ref[...].astype(f32)
-    for s in range(N_TP):
-        pieces[s] = flat[pl.ds(s, ROWS, stride=N_TP), :].astype(bf16)
-
-    def wide(first):
-        return jnp.concatenate([pieces[first + s] for s in range(N_TP // 2)], axis=1)
-
-    x_mine = wide(core * (N_TP // 2))
-    x_other = wide((1 - core) * (N_TP // 2))
-    mine = (0, 1, 2, 3)
-    other = (6, 7, 4, 5)
-    nt, nn = ((1,), (1,)), ((1,), (0,))
+    x = jnp.concatenate(
+        [flat[pl.ds(s, ROWS, stride=N_TP), :].astype(bf16) for s in range(N_TP)], axis=1
+    )
     for copy in copies:
         copy.wait()
-
-    def project(w):
-        w_mine = jnp.concatenate([held[i, w] for i in mine], axis=0)
-        w_other = jnp.concatenate([held[i, w] for i in other], axis=0)
-        return dot(x_mine, w_mine, nt) + dot(x_other, w_other, nt)
-
-    inner = (silu(project(0)) * project(1)).astype(bf16)
-    for side, slots in ((core, mine), (1 - core, other)):
-        w = jnp.concatenate([held[i, 2] for i in slots], axis=0)
-        part = dot(inner, w, nn)
-        for s in range(N_TP // 2):
-            flat[pl.ds(side * (N_TP // 2) + s, ROWS, stride=N_TP), :] = part[
-                :, s * LANES : (s + 1) * LANES
-            ]
+    wide = held[0:2].reshape(2 * N_Q * UNITS, N_TP * LANES)
+    both = dot(x, wide, ((1,), (1,)))
+    inner = (silu(both[:, : N_Q * UNITS]) * both[:, N_Q * UNITS :]).astype(bf16)
+    part = dot(inner, held[2], ((1,), (0,)))
+    for s in range(N_TP):
+        flat[pl.ds(s, ROWS, stride=N_TP), :] = part[:, s * LANES : (s + 1) * LANES]
     out_ref[...] = flat[...].astype(bf16)
 
 
@@ -158,6 +139,8 @@
 VMEM = pl.BlockSpec(memory_space=pltpu.VMEM)
 SMEM = pl.BlockSpec(memory_space=pltpu.SMEM)
 ANY = pl.BlockSpec(memory_space=pl.ANY)
+FREE = pl.BlockSpec(memory_space=pl.ANY)
+LOAD = pl.BlockSpec(memory_space=pltpu.VMEM)
 
 
 def call(body, ins, outs, *args, scratch=(), limit=4):
@@ -195,9 +178,9 @@
     shared_up,
     shared_down,
 ):
-    core, y, x = lax.axis_index("c"), lax.axis_index("y"), lax.axis_index("x")
+    y, x = lax.axis_index("y"), lax.axis_index("x")
     place = 2 * (y % 2) + x % 2
-    copies = call(copies_body, [VMEM], shape((N_TP, TOK, LANES)), hidden)
+    copies = call(copies_body, [LOAD], shape((N_TP, TOK, LANES)), hidden)
     tokens = lax.all_to_all(copies, ("y", "x"), 0, 0, tiled=True)
     select, combine = call(
         tables_body,
@@ -208,30 +191,26 @@
         routes,
         route_weights,
     )
-    order = jnp.bitwise_xor(place, jnp.arange(4, dtype=jnp.int32))
     pieces = call(
         weights_body,
         [SMEM, ANY, ANY, ANY],
-        [shape((3, UNITS, HALF))] * 4,
-        order,
+        [shape((3, UNITS, N_TP * LANES))] * 2,
+        (place % 2).reshape(1).astype(jnp.int32),
         gate_weight,
         up_weight,
         down_weight,
-        scratch=[pltpu.SemaphoreType.DMA((4, 3))],
-    )
-    mine = []
+        scratch=[pltpu.SemaphoreType.DMA((2, 3))],
+    )
+    mine, other = [], []
     for m, piece in enumerate(pieces):
         pairs = []
         for c in range(N_C):
             for j in range(N_TP):
                 sy, sx = j // N_X, j % N_X
-                v = (2 * (sy % 2) + sx % 2) ^ m
-                target = (v // 2) * N_TP + (sy - sy % 2 + c) * N_X + (sx - sx % 2 + v % 2)
+                target = (sy % 2) * N_TP + (sy - sy % 2 + c) * N_X + (sx - sx % 2 + (sx + m) % 2)
                 pairs.append((c * N_TP + j, target))
         mine.append(lax.ppermute(piece, ("c", "y", "x"), pairs))
-    other = []
-    for piece in mine:
-        other.append(lax.ppermute(piece, "c", [(0, 1), (1, 0)]))
+        other.append(lax.ppermute(mine[-1], "c", [(0, 1), (1, 0)]))
     flat = pltpu.VMEM((ROWS * N_TP, LANES), f32)
     own, packed = call(
         norm_body,
@@ -254,17 +233,15 @@
     )
     parts = call(
         experts_body,
-        [SMEM, VMEM] + [ANY] * 8,
+        [VMEM] + [FREE] * 4,
         shape((ROWS * N_TP, LANES)),
-        core.reshape(1).astype(jnp.int32),
         arrived.reshape(ROWS * N_TP, LANES),
         *mine,
         *other,
         scratch=[
             flat,
-            pltpu.VMEM((N_TP, ROWS, LANES), bf16),
-            pltpu.VMEM((8, 3, UNITS, HALF), bf16),
-            pltpu.SemaphoreType.DMA((8,)),
+            pltpu.VMEM((3, N_Q * UNITS, N_TP * LANES), bf16),
+            pltpu.SemaphoreType.DMA((4,)),
         ],
         limit=24,
     )

time: 114 us -> 106 us (0.930)
  starting transfers between devices: 54.7 us -> 39 us
  waiting for transfers between devices: 31.3 us -> 39 us
  Pallas kernels: 9.67 us -> 8.06 us
  blocking collectives: 13.9 us -> 15.2 us
    all_to_all x1, waiting for transfers between devices: 0.01 us -> 12.9 us  [per_device(): lax.all_to_all(packed.reshape(N_Z, CAP * N_TP, LANES), 'z', 0, 0, tiled=T...]
    all_to_all x1, starting transfers between devices: 9.76 us -> 3.61 us  [per_device(): lax.all_to_all(parts.reshape(N_Z, CAP * N_TP, LANES), 'z', 0, 0, tiled=True)]
    ppermute x4 -> x2, starting transfers between devices: 9.83 us -> 4.11 us  [per_device(): mine.append(lax.ppermute(piece, ('c', 'y', 'x'), pairs))]
    ppermute x4 -> x2, starting transfers between devices: 10.3 us -> 5.09 us  [per_device(): other.append(lax.ppermute(mine[-1], 'c', [(0, 1), (1, 0)]))]
    ppermute x4 -> x2, waiting for transfers between devices: 4.47 us -> 0.01 us  [per_device(): mine.append(lax.ppermute(piece, ('c', 'y', 'x'), pairs))]
    all_to_all x1, waiting for transfers between devices: 8.79 us -> 11.6 us  [per_device(): tokens = lax.all_to_all(copies, ('y', 'x'), 0, 0, tiled=True)]
    all_to_all x1, waiting for transfers between devices: 16.8 us -> 14.6 us  [per_device(): lax.all_to_all(parts.reshape(N_Z, CAP * N_TP, LANES), 'z', 0, 0, tiled=True)]
    pallas_call x8, Pallas kernels: 9.67 us -> 8.06 us  [call(): pl.pallas_call(body, in_specs=ins, out_specs=[VMEM] * len(shapes), out_sh...]
  transfers between devices with their start and end apart: 11 -> 7, of which waited for: 6 -> 3; matrix products, arithmetic and copies ran while one was open for 0% -> 0% of each run, Pallas kernels for 2% -> 3%
where the time goes in v2:
time: 106 us; the launch traced here: 105 us
  starting transfers between devices  39 us (37%)
  waiting for transfers between devices  39 us (37%)
  blocking collectives  15.2 us (14%)
  Pallas kernels  8.06 us (8%)
  local copies, waits for them, and re-layouts  3.86 us (4%)
    all_to_all x1, blocking collectives, per_device(): mixed = lax.all_to_all(mixed, ('y', 'x'), 0, 0, tiled=True)  15.2 us
    all_to_all x1, starting transfers between devices, per_device(): lax.all_to_all(packed.reshape(N_Z, CAP * N_TP, LANES), 'z', 0, 0, tiled=T...  14.8 us
    all_to_all x1, waiting for transfers between devices, per_device(): lax.all_to_all(parts.reshape(N_Z, CAP * N_TP, LANES), 'z', 0, 0, tiled=True)  14.6 us
    all_to_all x1, waiting for transfers between devices, per_device(): lax.all_to_all(packed.reshape(N_Z, CAP * N_TP, LANES), 'z', 0, 0, tiled=T...  12.9 us
    all_to_all x1, waiting for transfers between devices, per_device(): tokens = lax.all_to_all(copies, ('y', 'x'), 0, 0, tiled=True)  11.6 us
    all_to_all x1, starting transfers between devices, per_device(): tokens = lax.all_to_all(copies, ('y', 'x'), 0, 0, tiled=True)  11.4 us
    pallas_call x8, Pallas kernels, call(): pl.pallas_call(body, in_specs=ins, out_specs=[VMEM] * len(shapes), out_sh...  8.06 us
    ppermute x2, starting transfers between devices, per_device(): other.append(lax.ppermute(mine[-1], 'c', [(0, 1), (1, 0)]))  5.09 us
  transfers between devices with their start and end apart: 7, of which 3 were waited for; matrix products, arithmetic and copies ran while one was open for 0% of the time, Pallas kernels for 3%

profile of v2, /device:TPU:64, one launch (start us, length us, event | category | flops | bytes accessed | tf_op | source)
XLA Modules:
  0.0 105.2 jit_solution(15725196726030834490)
XLA Ops:
  0.0 1.4 %shard_map.103 = (bf16[3,32,4096]{2,1,0:T(8,128)(2,1)S(1)}, bf16[3,32,4096]{2,1,0:T(8,128)(2,1)S(1)}) custom-call(s32[1]{0:T(128)} %bitcast.5.first_ref, bf16[2,32,4096]{2,1,0:T(8,128)(2,1)} %gate_ref.2, bf16[2,32,4096]{2,1,0:T(8,128)(2,1)} %up_ref.2, bf16[2,32,4096]{2,1,0:T(8,128)(2,1)} %down_ref.2), custom_call_target="tpu_custom_call" | custom-call | tf_op jit(solution)/shard_map/pallas_call | solution.py:154
  1.4 0.7 collective-permute-start
  2.1 3.4 %collective-permute-start.1 = (bf16[3,32,4096]{2,1,0:T(8,128)(2,1)S(1)}, bf16[3,32,4096]{2,1,0:T(8,128)(2,1)S(1)}, u32[]{:S(2)}, u32[]{:S(2)}) collective-permute-start(bf16[3,32,4096]{2,1,0:T(8,128)(2,1)S(1)} %get-tuple-element.14), channel_id=1, source_target_pairs={{0,1},{1,0},{2,3},{3,2},{4,33},{5,32},{6,35},{7,34},{8,9},{9,8},{1... | collective-permute-start | bytes 2359304 | tf_op jit(solution)/shard_map/ppermute | solution.py:212
  5.6 0.7 shard_map.100
  6.2 11.4 %all-to-all-start = ((bf16[32,16,128]{2,1,0:T(8,128)(2,1)}), bf16[32,16,128]{2,1,0:T(8,128)(2,1)S(1)}, u32[]{:S(2)}, u32[]{:S(2)}) async-start(bf16[32,16,128]{2,1,0:T(8,128)(2,1)} %shard_map.100), calls=%async_computation | async-start | bytes 262144 | tf_op jit(solution)/shard_map/all_to_all | solution.py:184
  17.6 0.1 copy.11.routes_ref
  17.7 0.6 copy-done.8
  18.4 0.2 shard_map.101
  18.6 11.6 %all-to-all-done.rows_ref = bf16[32,16,128]{2,1,0:T(8,128)(2,1)S(1)} async-done(((bf16[32,16,128]{2,1,0:T(8,128)(2,1)}), bf16[32,16,128]{2,1,0:T(8,128)(2,1)S(1)}, u32[]{:S(2)}, u32[]{:S(2)}) %all-to-all-start) | async-done | bytes 131104 | tf_op jit(solution)/shard_map/all_to_all | solution.py:184
  30.2 1.4 %shard_map.102 = (bf16[16,4096]{1,0:T(8,128)(2,1)S(1)}, bf16[1152,128]{1,0:T(8,128)(2,1)}) custom-call(bf16[32,16,128]{2,1,0:T(8,128)(2,1)S(1)} %all-to-all-done.rows_ref, f32[32,1,128]{2,1,0:T(1,128)S(1)} %bitcast.10, bf16[40,16]{1,0:T(8,128)(2,1)S(1)} %get-tuple-element.11.select_ref), custom_call_target="tpu_custom_call" | custom-call | tf_op jit(solution)/shard_map/pallas_call | solution.py:154
  31.6 0.6 copy-done.3
  32.2 14.8 %all-to-all-start.1 = ((bf16[12,96,128]{2,1,0:T(8,128)(2,1)}), bf16[12,96,128]{2,1,0:T(8,128)(2,1)S(1)}, u32[]{:S(2)}, u32[]{:S(2)}) async-start(bf16[12,96,128]{2,1,0:T(8,128)(2,1)} %bitcast.3), calls=%async_computation.1 | async-start | bytes 589824 | tf_op jit(solution)/shard_map/all_to_all | solution.py:224
  47.0 3.2 %collective-permute-start.2 = (bf16[3,32,4096]{2,1,0:T(8,128)(2,1)S(1)}, bf16[3,32,4096]{2,1,0:T(8,128)(2,1)S(1)}, u32[]{:S(2)}, u32[]{:S(2)}) collective-permute-start(bf16[3,32,4096]{2,1,0:T(8,128)(2,1)S(1)} %collective-permute-done.g0), channel_id=1, source_target_pairs={{0,32},{32,0},{1,33},{33,1},{2,34},{34,2},{3,35},{35,3},{4,36},{36... | collective-permute-start | bytes 2359304 | tf_op jit(solution)/shard_map/ppermute | solution.py:213
  50.2 1.9 %collective-permute-start.3 = (bf16[3,32,4096]{2,1,0:T(8,128)(2,1)S(1)}, bf16[3,32,4096]{2,1,0:T(8,128)(2,1)S(1)}, u32[]{:S(2)}, u32[]{:S(2)}) collective-permute-start(bf16[3,32,4096]{2,1,0:T(8,128)(2,1)S(1)} %collective-permute-done.1.g1), channel_id=1, source_target_pairs={{0,32},{32,0},{1,33},{33,1},{2,34},{34,2},{3,35},{35,3},{4,36},{36... | collective-permute-start | bytes 2359304 | tf_op jit(solution)/shard_map/ppermute | solution.py:213
  52.1 12.9 %all-to-all-done.1 = bf16[12,96,128]{2,1,0:T(8,128)(2,1)S(1)} async-done(((bf16[12,96,128]{2,1,0:T(8,128)(2,1)}), bf16[12,96,128]{2,1,0:T(8,128)(2,1)S(1)}, u32[]{:S(2)}, u32[]{:S(2)}) %all-to-all-start.1) | async-done | bytes 294944 | tf_op jit(solution)/shard_map/all_to_all | solution.py:224
  65.0 3.1 %shard_map.104 = bf16[1152,128]{1,0:T(8,128)(2,1)} custom-call(bf16[1152,128]{1,0:T(8,128)(2,1)S(1)} %bitcast.8, bf16[3,32,4096]{2,1,0:T(8,128)(2,1)S(1)} %collective-permute-done.g0, bf16[3,32,4096]{2,1,0:T(8,128)(2,1)S(1)} %collective-permute-done.1.g1, bf16[3,32,4096]{2,1,0:T(8,128)(2,1)S(1)} %collective-permute-done.2.g2, ...), custom_call_target="tpu_custom_call" | custom-call | tf_op jit(solution)/shard_map/pallas_call | solution.py:154
  68.1 3.6 %all-to-all-start.2 = ((bf16[12,96,128]{2,1,0:T(8,128)(2,1)}), bf16[12,96,128]{2,1,0:T(8,128)(2,1)S(1)}, u32[]{:S(2)}, u32[]{:S(2)}) async-start(bf16[12,96,128]{2,1,0:T(8,128)(2,1)} %bitcast.6), calls=%async_computation.2 | async-start | bytes 589824 | tf_op jit(solution)/shard_map/all_to_all | solution.py:248
  71.8 0.9 copy-done.2
  72.7 0.9 copy-done.4
  73.6 0.4 shard_map.105.shared_ref
  74.0 14.6 %all-to-all-done.2 = bf16[12,96,128]{2,1,0:T(8,128)(2,1)S(1)} async-done(((bf16[12,96,128]{2,1,0:T(8,128)(2,1)}), bf16[12,96,128]{2,1,0:T(8,128)(2,1)S(1)}, u32[]{:S(2)}, u32[]{:S(2)}) %all-to-all-start.2) | async-done | bytes 294944 | tf_op jit(solution)/shard_map/all_to_all | solution.py:248
  88.6 0.8 shard_map.106
  89.4 15.2 %all_to_all.20.parts_ref = bf16[32,16,128]{2,1,0:T(8,128)(2,1)S(1)} all-to-all(bf16[32,16,128]{2,1,0:T(8,128)(2,1)S(1)} %shard_map.106), channel_id=1, replica_groups=mesh['z'=12,'c'=2,'y'=8,'x'=4] {'y','x'}, dimensions={0} | all-to-all | bytes 262144 | tf_op jit(solution)/shard_map/all_to_all | solution.py:258
  104.6 0.6 copy.13
  (20 shorter events, 0.2 us)
Async XLA Ops:
  0.0 5.5 %copy-start.7 = (bf16[16,128]{1,0:T(8,128)(2,1)S(1)}, bf16[16,128]{1,0:T(8,128)(2,1)}, u32[]{:S(2)}) copy-start(bf16[16,128]{1,0:T(8,128)(2,1)} %hidden_ref.1) | copy-start | bytes 12292
  1.4 45.6 %collective-permute-start = (bf16[3,32,4096]{2,1,0:T(8,128)(2,1)S(1)}, bf16[3,32,4096]{2,1,0:T(8,128)(2,1)S(1)}, u32[]{:S(2)}, u32[]{:S(2)}) collective-permute-start(bf16[3,32,4096]{2,1,0:T(8,128)(2,1)S(1)} %get-tuple-element.13), channel_id=1, source_target_pairs={{0,0},{1,1},{2,2},{3,3},{4,32},{5,33},{6,34},{7,35},{8,8},{9,9},{1... | collective-permute-start | bytes 2359304 | tf_op jit(solution)/shard_map/ppermute | solution.py:212
  2.1 48.0 %collective-permute-start.1 = (bf16[3,32,4096]{2,1,0:T(8,128)(2,1)S(1)}, bf16[3,32,4096]{2,1,0:T(8,128)(2,1)S(1)}, u32[]{:S(2)}, u32[]{:S(2)}) collective-permute-start(bf16[3,32,4096]{2,1,0:T(8,128)(2,1)S(1)} %get-tuple-element.14), channel_id=1, source_target_pairs={{0,1},{1,0},{2,3},{3,2},{4,33},{5,32},{6,35},{7,34},{8,9},{9,8},{1... | collective-permute-start | bytes 2359304 | tf_op jit(solution)/shard_map/ppermute | solution.py:212
  6.2 11.4 %copy-start.6 = (s32[16,4]{0,1:T(4,128)S(1)}, s32[16,4]{0,1:T(4,128)}, u32[]{:S(2)}) copy-start(s32[16,4]{0,1:T(4,128)} %param.12) | copy-start | bytes 772
  6.2 23.9 %all-to-all-start = ((bf16[32,16,128]{2,1,0:T(8,128)(2,1)}), bf16[32,16,128]{2,1,0:T(8,128)(2,1)S(1)}, u32[]{:S(2)}, u32[]{:S(2)}) async-start(bf16[32,16,128]{2,1,0:T(8,128)(2,1)} %shard_map.100), calls=%async_computation | async-start | bytes 262144 | tf_op jit(solution)/shard_map/all_to_all | solution.py:184
  17.6 0.7 copy-start.8
  18.3 11.8 %copy-start.5 = (f32[4096]{0:T(1024)S(1)}, f32[4096]{0:T(1024)}, u32[]{:S(2)}) copy-start(f32[4096]{0:T(1024)} %param.11) | copy-start | bytes 49156
  31.6 0.6 copy-start.3
  32.2 32.8 %all-to-all-start.1 = ((bf16[12,96,128]{2,1,0:T(8,128)(2,1)}), bf16[12,96,128]{2,1,0:T(8,128)(2,1)S(1)}, u32[]{:S(2)}, u32[]{:S(2)}) async-start(bf16[12,96,128]{2,1,0:T(8,128)(2,1)} %bitcast.3), calls=%async_computation.1 | async-start | bytes 589824 | tf_op jit(solution)/shard_map/all_to_all | solution.py:224
  47.0 18.0 %collective-permute-start.2 = (bf16[3,32,4096]{2,1,0:T(8,128)(2,1)S(1)}, bf16[3,32,4096]{2,1,0:T(8,128)(2,1)S(1)}, u32[]{:S(2)}, u32[]{:S(2)}) collective-permute-start(bf16[3,32,4096]{2,1,0:T(8,128)(2,1)S(1)} %collective-permute-done.g0), channel_id=1, source_target_pairs={{0,32},{32,0},{1,33},{33,1},{2,34},{34,2},{3,35},{35,3},{4,36},{36... | collective-permute-start | bytes 2359304 | tf_op jit(solution)/shard_map/ppermute | solution.py:213
  50.2 14.8 %collective-permute-start.3 = (bf16[3,32,4096]{2,1,0:T(8,128)(2,1)S(1)}, bf16[3,32,4096]{2,1,0:T(8,128)(2,1)S(1)}, u32[]{:S(2)}, u32[]{:S(2)}) collective-permute-start(bf16[3,32,4096]{2,1,0:T(8,128)(2,1)S(1)} %collective-permute-done.1.g1), channel_id=1, source_target_pairs={{0,32},{32,0},{1,33},{33,1},{2,34},{34,2},{3,35},{35,3},{4,36},{36... | collective-permute-start | bytes 2359304 | tf_op jit(solution)/shard_map/ppermute | solution.py:213
  68.1 3.6 %copy-start = (bf16[32,4096]{1,0:T(8,128)(2,1)S(1)}, bf16[32,4096]{1,0:T(8,128)(2,1)}, u32[]{:S(2)}) copy-start(bf16[32,4096]{1,0:T(8,128)(2,1)} %gate_ref.3) | copy-start | bytes 786436
  68.1 3.6 %copy-start.1 = (bf16[32,4096]{1,0:T(8,128)(2,1)S(1)}, bf16[32,4096]{1,0:T(8,128)(2,1)}, u32[]{:S(2)}) copy-start(bf16[32,4096]{1,0:T(8,128)(2,1)} %up_ref.3) | copy-start | bytes 786436
  68.1 20.5 %all-to-all-start.2 = ((bf16[12,96,128]{2,1,0:T(8,128)(2,1)}), bf16[12,96,128]{2,1,0:T(8,128)(2,1)S(1)}, u32[]{:S(2)}, u32[]{:S(2)}) async-start(bf16[12,96,128]{2,1,0:T(8,128)(2,1)} %bitcast.6), calls=%async_computation.2 | async-start | bytes 589824 | tf_op jit(solution)/shard_map/all_to_all | solution.py:248
  71.8 1.0 copy-start.2
  72.7 0.9 copy-start.4

commit v3 on v2

--- a/solution.py
+++ b/solution.py
@@ -30,9 +30,13 @@
     return lax.dot_general(a, b, (dims, ((), ())), preferred_element_type=f32, precision=precision)
 
 
-def copies_body(hidden_ref, out_ref):
+def copies_body(hidden_ref, out_ref, own, sem):
+    copy = pltpu.make_async_copy(hidden_ref, own, sem)
+    copy.start()
+    copy.wait()
+    value = own[...]
     for j in range(N_TP):
-        out_ref[j] = hidden_ref[...]
+        out_ref[j] = value
 
 
 def slot_of(shape, dim):
@@ -41,7 +45,8 @@
     return block, (row - CAP * block).astype(f32)
 
 
-def tables_body(place_ref, across_ref, routes_ref, weights_ref, select_ref, combine_ref):
+def tables_body(place_ref, across_ref, routes_ref, weights_ref, gain_ref, select_ref, combine_ref, kept_ref):
+    kept_ref[...] = gain_ref[...]
     place = place_ref[0]
     block, wanted = slot_of((PADDED, TOK), 0)
     named = jnp.zeros((PADDED, TOK), f32)
@@ -59,21 +64,31 @@
         total = total + jnp.where(hit, weights_ref[:, k : k + 1], 0.0)
     earlier = jnp.where(iota((TOK, TOK), 1) < iota((TOK, TOK), 0), 1.0, 0.0).astype(bf16)
     rank = dot(earlier, named.astype(bf16), ((1,), (0,)))
-    combine_ref[...] = jnp.where(rank == wanted, total, 0.0)
-
-
-def norm_body(rows_ref, gain_ref, select_ref, own_ref, out_ref, flat):
+    left = jnp.where(rank == wanted, total, 0.0)
+    for n in range(3):
+        term = left.astype(bf16)
+        combine_ref[n * TOK : (n + 1) * TOK, :] = term
+        left = left - term.astype(f32)
+
+
+def norm_body(rows_ref, gain_ref, select_ref, own_ref, out_ref, flat, kept, sem):
     squares = jnp.zeros((TOK, LANES), f32)
     for s in range(N_TP):
         v = rows_ref[s].astype(f32)
         squares = squares + v * v
     inv = lax.rsqrt(jnp.sum(squares, axis=1, keepdims=True) * (1.0 / (N_TP * LANES)) + norm_eps)
+    for s in range(N_TP):
+        kept[:, s * LANES : (s + 1) * LANES] = (
+            rows_ref[s].astype(f32) * inv * gain_ref[s : s + 1, :]
+        ).astype(bf16)
+    copy = pltpu.make_async_copy(kept, own_ref, sem)
+    copy.start()
     select = select_ref[...]
     for s in range(N_TP):
-        piece = (rows_ref[s].astype(f32) * inv * gain_ref[s]).astype(bf16)
-        own_ref[:, s * LANES : (s + 1) * LANES] = piece
+        piece = kept[:, s * LANES : (s + 1) * LANES]
         flat[pl.ds(s, ROWS, stride=N_TP), :] = dot(select, piece, ((1,), (0,)))[0:ROWS]
     out_ref[...] = flat[...].astype(bf16)
+    copy.wait()
 
 
 def weights_body(first_ref, gate_ref, up_ref, down_ref, o0, o1, sems):
@@ -98,25 +113,25 @@
     out_ref[...] = dot(inner, down_ref[...], ((1,), (0,)))
 
 
-def experts_body(rows_ref, g0, g1, g2, g3, out_ref, flat, held, sems):
-    copies = [
-        pltpu.make_async_copy(ref, held.at[:, pl.ds(i * UNITS, UNITS)], sems.at[i])
-        for i, ref in enumerate((g0, g1, g2, g3))
-    ]
-    for copy in copies:
-        copy.start()
+def experts_body(rows_ref, g0, g1, g2, g3, out_ref, flat):
+    given = (g0, g1, g2, g3)
     flat[...] = rows_ref[...].astype(f32)
-    x = jnp.concatenate(
-        [flat[pl.ds(s, ROWS, stride=N_TP), :].astype(bf16) for s in range(N_TP)], axis=1
-    )
-    for copy in copies:
-        copy.wait()
-    wide = held[0:2].reshape(2 * N_Q * UNITS, N_TP * LANES)
-    both = dot(x, wide, ((1,), (1,)))
+    wide = 2 * LANES
+    both = jnp.zeros((ROWS, 2 * N_Q * UNITS), f32)
+    for n in range(N_TP // 2):
+        x = jnp.concatenate(
+            [flat[pl.ds(2 * n + h, ROWS, stride=N_TP), :].astype(bf16) for h in range(2)], axis=1
+        )
+        w = jnp.concatenate(
+            [ref[p, :, n * wide : (n + 1) * wide] for p in range(2) for ref in given], axis=0
+        )
+        both = both + dot(x, w, ((1,), (1,)))
     inner = (silu(both[:, : N_Q * UNITS]) * both[:, N_Q * UNITS :]).astype(bf16)
-    part = dot(inner, held[2], ((1,), (0,)))
-    for s in range(N_TP):
-        flat[pl.ds(s, ROWS, stride=N_TP), :] = part[:, s * LANES : (s + 1) * LANES]
+    for n in range(N_TP // 2):
+        w = jnp.concatenate([ref[2, :, n * wide : (n + 1) * wide] for ref in given], axis=0)
+        part = dot(inner, w, ((1,), (0,)))
+        for h in range(2):
+            flat[pl.ds(2 * n + h, ROWS, stride=N_TP), :] = part[:, h * LANES : (h + 1) * LANES]
     out_ref[...] = flat[...].astype(bf16)
 
 
@@ -124,8 +139,9 @@
     flat[...] = rows_ref[...].astype(f32)
     combine = combine_ref[:, 0:ROWS]
     for s in range(N_TP):
-        piece = flat[pl.ds(s, ROWS, stride=N_TP), :]
-        total = dot(combine, piece, ((1,), (0,)), lax.Precision.HIGHEST)
+        piece = flat[pl.ds(s, ROWS, stride=N_TP), :].astype(bf16)
+        terms = dot(combine, piece, ((1,), (0,)))
+        total = terms[0:TOK] + terms[TOK : 2 * TOK] + terms[2 * TOK : 3 * TOK]
         out_ref[s] = (total + shared_ref[:, s * LANES : (s + 1) * LANES]).astype(bf16)
 
 
@@ -139,11 +155,9 @@
 VMEM = pl.BlockSpec(memory_space=pltpu.VMEM)
 SMEM = pl.BlockSpec(memory_space=pltpu.SMEM)
 ANY = pl.BlockSpec(memory_space=pl.ANY)
-FREE = pl.BlockSpec(memory_space=pl.ANY)
-LOAD = pl.BlockSpec(memory_space=pltpu.VMEM)
-
-
-def call(body, ins, outs, *args, scratch=(), limit=4):
+
+
+def call(body, ins, outs, *args, scratch=(), limit=4, outspecs=None):
     single = not isinstance(outs, list)
     shapes = [outs] if single else outs
     spaces = {id(VMEM): pltpu.VMEM, id(ANY): pltpu.HBM}
@@ -154,7 +168,7 @@
     got = pl.pallas_call(
         body,
         in_specs=ins,
-        out_specs=[VMEM] * len(shapes),
+        out_specs=outspecs or [VMEM] * len(shapes),
         out_shape=shapes,
         scratch_shapes=list(scratch),
         compiler_params=pltpu.CompilerParams(vmem_limit_bytes=limit << 20),
@@ -180,16 +194,23 @@
 ):
     y, x = lax.axis_index("y"), lax.axis_index("x")
     place = 2 * (y % 2) + x % 2
-    copies = call(copies_body, [LOAD], shape((N_TP, TOK, LANES)), hidden)
+    copies = call(
+        copies_body,
+        [ANY],
+        shape((N_TP, TOK, LANES)),
+        hidden,
+        scratch=[pltpu.VMEM((TOK, LANES), bf16), pltpu.SemaphoreType.DMA],
+    )
     tokens = lax.all_to_all(copies, ("y", "x"), 0, 0, tiled=True)
-    select, combine = call(
+    select, combine, gain = call(
         tables_body,
-        [SMEM] + [VMEM] * 3,
-        [shape((PADDED, TOK)), shape((TOK, PADDED), f32)],
+        [SMEM] + [VMEM] * 4,
+        [shape((PADDED, TOK)), shape((3 * TOK, PADDED)), shape((N_TP, LANES), f32)],
         place.reshape(1).astype(jnp.int32),
         routes.T,
         routes,
         route_weights,
+        norm_gain.reshape(N_TP, LANES),
     )
     pieces = call(
         weights_body,
@@ -215,11 +236,12 @@
     own, packed = call(
         norm_body,
         [VMEM] * 3,
-        [shape((TOK, N_TP * LANES)), shape((ROWS * N_TP, LANES))],
+        [pltpu.HBM((TOK, N_TP * LANES), bf16), shape((ROWS * N_TP, LANES))],
         tokens,
-        norm_gain.reshape(N_TP, 1, LANES),
+        gain,
         select,
-        scratch=[flat],
+        scratch=[flat, pltpu.VMEM((TOK, N_TP * LANES), bf16), pltpu.SemaphoreType.DMA],
+        outspecs=[ANY, VMEM],
     )
     arrived = lax.all_to_all(packed.reshape(N_Z, CAP * N_TP, LANES), "z", 0, 0, tiled=True)
     shared = call(
@@ -233,17 +255,13 @@
     )
     parts = call(
         experts_body,
-        [VMEM] + [FREE] * 4,
+        [VMEM] * 5,
         shape((ROWS * N_TP, LANES)),
         arrived.reshape(ROWS * N_TP, LANES),
         *mine,
         *other,
-        scratch=[
-            flat,
-            pltpu.VMEM((3, N_Q * UNITS, N_TP * LANES), bf16),
-            pltpu.SemaphoreType.DMA((4,)),
-        ],
-        limit=24,
+        scratch=[flat],
+        limit=8,
     )
     returned = lax.all_to_all(parts.reshape(N_Z, CAP * N_TP, LANES), "z", 0, 0, tiled=True)
     mixed = call(
@@ -256,7 +274,7 @@
         scratch=[flat],
     )
     mixed = lax.all_to_all(mixed, ("y", "x"), 0, 0, tiled=True)
-    return call(sum_body, [VMEM], shape((TOK, LANES)), mixed)
+    return call(sum_body, [VMEM], jax.ShapeDtypeStruct((TOK, LANES), bf16), mixed)
 
 
 def solution(mesh):

time: 106 us -> 104 us (0.981)
  local copies, waits for them, and re-layouts: 3.86 us -> 2.58 us
    unnamed x21 -> x16, local copies, waits for them, and re-layouts: 3.86 us -> 2.58 us
  transfers between devices with their start and end apart: 7 -> 7, of which waited for: 3 -> 3; matrix products, arithmetic and copies ran while one was open for 0% -> 0% of each run, Pallas kernels for 3% -> 4%
where the time goes in v3:
time: 104 us
  starting transfers between devices  38.9 us (37%)
  waiting for transfers between devices  38.4 us (37%)
  blocking collectives  15 us (14%)
  Pallas kernels  8.46 us (8%)
  local copies, waits for them, and re-layouts  2.58 us (2%)
    all_to_all x1, blocking collectives, per_device(): mixed = lax.all_to_all(mixed, ('y', 'x'), 0, 0, tiled=True)  15 us
    all_to_all x1, starting transfers between devices, per_device(): lax.all_to_all(packed.reshape(N_Z, CAP * N_TP, LANES), 'z', 0, 0, tiled=T...  14.8 us
    all_to_all x1, waiting for transfers between devices, per_device(): lax.all_to_all(parts.reshape(N_Z, CAP * N_TP, LANES), 'z', 0, 0, tiled=True)  14.6 us
    all_to_all x1, waiting for transfers between devices, per_device(): lax.all_to_all(packed.reshape(N_Z, CAP * N_TP, LANES), 'z', 0, 0, tiled=T...  12.9 us
    all_to_all x1, starting transfers between devices, per_device(): tokens = lax.all_to_all(copies, ('y', 'x'), 0, 0, tiled=True)  11.3 us
    all_to_all x1, waiting for transfers between devices, per_device(): tokens = lax.all_to_all(copies, ('y', 'x'), 0, 0, tiled=True)  11 us
    pallas_call x8, Pallas kernels, call(): pl.pallas_call(body, in_specs=ins, out_specs=outspecs or [VMEM] * len(sha...  8.46 us
    ppermute x2, starting transfers between devices, per_device(): other.append(lax.ppermute(mine[-1], 'c', [(0, 1), (1, 0)]))  5.09 us
  transfers between devices with their start and end apart: 7, of which 3 were waited for; matrix products, arithmetic and copies ran while one was open for 0% of the time, Pallas kernels for 4%

profile of v3, /device:TPU:64, one launch (start us, length us, event | category | flops | bytes accessed | tf_op | source)
XLA Modules:
  0.0 103.5 jit_solution(12254975880260568666)
XLA Ops:
  0.0 1.4 %shard_map.103 = (bf16[3,32,4096]{2,1,0:T(8,128)(2,1)S(1)}, bf16[3,32,4096]{2,1,0:T(8,128)(2,1)S(1)}) custom-call(s32[1]{0:T(128)} %bitcast.5.first_ref, bf16[2,32,4096]{2,1,0:T(8,128)(2,1)} %gate_ref.2, bf16[2,32,4096]{2,1,0:T(8,128)(2,1)} %up_ref.2, bf16[2,32,4096]{2,1,0:T(8,128)(2,1)} %down_ref.2), custom_call_target="tpu_custom_call" | custom-call | tf_op jit(solution)/shard_map/pallas_call | solution.py:168
  1.4 0.7 collective-permute-start
  2.1 3.4 %collective-permute-start.1 = (bf16[3,32,4096]{2,1,0:T(8,128)(2,1)S(1)}, bf16[3,32,4096]{2,1,0:T(8,128)(2,1)S(1)}, u32[]{:S(2)}, u32[]{:S(2)}) collective-permute-start(bf16[3,32,4096]{2,1,0:T(8,128)(2,1)S(1)} %get-tuple-element.16), channel_id=1, source_target_pairs={{0,1},{1,0},{2,3},{3,2},{4,33},{5,32},{6,35},{7,34},{8,9},{9,8},{1... | collective-permute-start | bytes 2359304 | tf_op jit(solution)/shard_map/ppermute | solution.py:233
  5.5 1.4 %shard_map.100 = bf16[32,16,128]{2,1,0:T(8,128)(2,1)} custom-call(bf16[16,128]{1,0:T(8,128)(2,1)} %hidden_ref.1), custom_call_target="tpu_custom_call" | custom-call | tf_op jit(solution)/shard_map/pallas_call | solution.py:168
  6.9 11.3 %all-to-all-start = ((bf16[32,16,128]{2,1,0:T(8,128)(2,1)}), bf16[32,16,128]{2,1,0:T(8,128)(2,1)S(1)}, u32[]{:S(2)}, u32[]{:S(2)}) async-start(bf16[32,16,128]{2,1,0:T(8,128)(2,1)} %shard_map.100), calls=%async_computation | async-start | bytes 262144 | tf_op jit(solution)/shard_map/all_to_all | solution.py:204
  18.2 0.1 copy.11.routes_ref
  18.3 0.1 copy.12.weights_ref
  18.4 0.5 copy-done.4
  18.9 0.2 shard_map.101
  19.1 11.0 %all-to-all-done.rows_ref = bf16[32,16,128]{2,1,0:T(8,128)(2,1)S(1)} async-done(((bf16[32,16,128]{2,1,0:T(8,128)(2,1)}), bf16[32,16,128]{2,1,0:T(8,128)(2,1)S(1)}, u32[]{:S(2)}, u32[]{:S(2)}) %all-to-all-start) | async-done | bytes 131104 | tf_op jit(solution)/shard_map/all_to_all | solution.py:204
  30.1 1.8 %shard_map.102 = (bf16[16,4096]{1,0:T(8,128)(2,1)}, bf16[1152,128]{1,0:T(8,128)(2,1)}) custom-call(bf16[32,16,128]{2,1,0:T(8,128)(2,1)S(1)} %all-to-all-done.rows_ref, f32[32,128]{1,0:T(8,128)S(1)} %get-tuple-element.12.gain_ref, bf16[40,16]{1,0:T(8,128)(2,1)S(1)} %get-tuple-element.13.select_ref), custom_call_target="tpu_custom_call" | custom-call | tf_op jit(solution)/shard_map/pallas_call | solution.py:168
  31.9 14.8 %all-to-all-start.1 = ((bf16[12,96,128]{2,1,0:T(8,128)(2,1)}), bf16[12,96,128]{2,1,0:T(8,128)(2,1)S(1)}, u32[]{:S(2)}, u32[]{:S(2)}) async-start(bf16[12,96,128]{2,1,0:T(8,128)(2,1)} %bitcast.3), calls=%async_computation.1 | async-start | bytes 589824 | tf_op jit(solution)/shard_map/all_to_all | solution.py:246
  46.7 3.2 %collective-permute-start.2 = (bf16[3,32,4096]{2,1,0:T(8,128)(2,1)S(1)}, bf16[3,32,4096]{2,1,0:T(8,128)(2,1)S(1)}, u32[]{:S(2)}, u32[]{:S(2)}) collective-permute-start(bf16[3,32,4096]{2,1,0:T(8,128)(2,1)S(1)} %collective-permute-done.g0), channel_id=1, source_target_pairs={{0,32},{32,0},{1,33},{33,1},{2,34},{34,2},{3,35},{35,3},{4,36},{36... | collective-permute-start | bytes 2359304 | tf_op jit(solution)/shard_map/ppermute | solution.py:234
  49.9 1.9 %collective-permute-start.3 = (bf16[3,32,4096]{2,1,0:T(8,128)(2,1)S(1)}, bf16[3,32,4096]{2,1,0:T(8,128)(2,1)S(1)}, u32[]{:S(2)}, u32[]{:S(2)}) collective-permute-start(bf16[3,32,4096]{2,1,0:T(8,128)(2,1)S(1)} %collective-permute-done.1.g1), channel_id=1, source_target_pairs={{0,32},{32,0},{1,33},{33,1},{2,34},{34,2},{3,35},{35,3},{4,36},{36... | collective-permute-start | bytes 2359304 | tf_op jit(solution)/shard_map/ppermute | solution.py:234
  51.8 12.9 %all-to-all-done.1 = bf16[12,96,128]{2,1,0:T(8,128)(2,1)S(1)} async-done(((bf16[12,96,128]{2,1,0:T(8,128)(2,1)}), bf16[12,96,128]{2,1,0:T(8,128)(2,1)S(1)}, u32[]{:S(2)}, u32[]{:S(2)}) %all-to-all-start.1) | async-done | bytes 294944 | tf_op jit(solution)/shard_map/all_to_all | solution.py:246
  64.7 2.2 %shard_map.104 = bf16[1152,128]{1,0:T(8,128)(2,1)} custom-call(bf16[1152,128]{1,0:T(8,128)(2,1)S(1)} %bitcast.8, bf16[3,32,4096]{2,1,0:T(8,128)(2,1)S(1)} %collective-permute-done.g0, bf16[3,32,4096]{2,1,0:T(8,128)(2,1)S(1)} %collective-permute-done.1.g1, bf16[3,32,4096]{2,1,0:T(8,128)(2,1)S(1)} %collective-permute-done.2.g2, ...), custom_call_target="tpu_custom_call" | custom-call | tf_op jit(solution)/shard_map/pallas_call | solution.py:168
  66.9 3.6 %all-to-all-start.2 = ((bf16[12,96,128]{2,1,0:T(8,128)(2,1)}), bf16[12,96,128]{2,1,0:T(8,128)(2,1)S(1)}, u32[]{:S(2)}, u32[]{:S(2)}) async-start(bf16[12,96,128]{2,1,0:T(8,128)(2,1)} %bitcast.6), calls=%async_computation.2 | async-start | bytes 589824 | tf_op jit(solution)/shard_map/all_to_all | solution.py:266
  70.5 0.9 copy-done.2
  71.5 0.9 copy-done.3
  72.4 0.4 shard_map.105.shared_ref
  72.8 14.6 %all-to-all-done.2 = bf16[12,96,128]{2,1,0:T(8,128)(2,1)S(1)} async-done(((bf16[12,96,128]{2,1,0:T(8,128)(2,1)}), bf16[12,96,128]{2,1,0:T(8,128)(2,1)S(1)}, u32[]{:S(2)}, u32[]{:S(2)}) %all-to-all-start.2) | async-done | bytes 294944 | tf_op jit(solution)/shard_map/all_to_all | solution.py:266
  87.3 0.5 shard_map.106
  87.9 15.0 %all_to_all.20.parts_ref = bf16[32,16,128]{2,1,0:T(8,128)(2,1)S(1)} all-to-all(bf16[32,16,128]{2,1,0:T(8,128)(2,1)S(1)} %shard_map.106), channel_id=1, replica_groups=mesh['z'=12,'c'=2,'y'=8,'x'=4] {'y','x'}, dimensions={0} | all-to-all | bytes 262144 | tf_op jit(solution)/shard_map/all_to_all | solution.py:276
  102.9 0.6 shard_map.107
  (15 shorter events, 0.0 us)
Async XLA Ops:
  1.4 45.3 %collective-permute-start = (bf16[3,32,4096]{2,1,0:T(8,128)(2,1)S(1)}, bf16[3,32,4096]{2,1,0:T(8,128)(2,1)S(1)}, u32[]{:S(2)}, u32[]{:S(2)}) collective-permute-start(bf16[3,32,4096]{2,1,0:T(8,128)(2,1)S(1)} %get-tuple-element.15), channel_id=1, source_target_pairs={{0,0},{1,1},{2,2},{3,3},{4,32},{5,33},{6,34},{7,35},{8,8},{9,9},{1... | collective-permute-start | bytes 2359304 | tf_op jit(solution)/shard_map/ppermute | solution.py:233
  2.1 47.7 %collective-permute-start.1 = (bf16[3,32,4096]{2,1,0:T(8,128)(2,1)S(1)}, bf16[3,32,4096]{2,1,0:T(8,128)(2,1)S(1)}, u32[]{:S(2)}, u32[]{:S(2)}) collective-permute-start(bf16[3,32,4096]{2,1,0:T(8,128)(2,1)S(1)} %get-tuple-element.16), channel_id=1, source_target_pairs={{0,1},{1,0},{2,3},{3,2},{4,33},{5,32},{6,35},{7,34},{8,9},{9,8},{1... | collective-permute-start | bytes 2359304 | tf_op jit(solution)/shard_map/ppermute | solution.py:233
  6.9 11.3 %copy-start.5 = (s32[16,4]{0,1:T(4,128)S(1)}, s32[16,4]{0,1:T(4,128)}, u32[]{:S(2)}) copy-start(s32[16,4]{0,1:T(4,128)} %param.12) | copy-start | bytes 772
  6.9 11.4 %copy-start.6 = (f32[16,4]{0,1:T(4,128)S(1)}, f32[16,4]{0,1:T(4,128)}, u32[]{:S(2)}) copy-start(f32[16,4]{0,1:T(4,128)} %param.13) | copy-start | bytes 772
  6.9 23.2 %all-to-all-start = ((bf16[32,16,128]{2,1,0:T(8,128)(2,1)}), bf16[32,16,128]{2,1,0:T(8,128)(2,1)S(1)}, u32[]{:S(2)}, u32[]{:S(2)}) async-start(bf16[32,16,128]{2,1,0:T(8,128)(2,1)} %shard_map.100), calls=%async_computation | async-start | bytes 262144 | tf_op jit(solution)/shard_map/all_to_all | solution.py:204
  18.2 0.7 copy-start.4
  31.9 32.8 %all-to-all-start.1 = ((bf16[12,96,128]{2,1,0:T(8,128)(2,1)}), bf16[12,96,128]{2,1,0:T(8,128)(2,1)S(1)}, u32[]{:S(2)}, u32[]{:S(2)}) async-start(bf16[12,96,128]{2,1,0:T(8,128)(2,1)} %bitcast.3), calls=%async_computation.1 | async-start | bytes 589824 | tf_op jit(solution)/shard_map/all_to_all | solution.py:246
  46.7 18.0 %collective-permute-start.2 = (bf16[3,32,4096]{2,1,0:T(8,128)(2,1)S(1)}, bf16[3,32,4096]{2,1,0:T(8,128)(2,1)S(1)}, u32[]{:S(2)}, u32[]{:S(2)}) collective-permute-start(bf16[3,32,4096]{2,1,0:T(8,128)(2,1)S(1)} %collective-permute-done.g0), channel_id=1, source_target_pairs={{0,32},{32,0},{1,33},{33,1},{2,34},{34,2},{3,35},{35,3},{4,36},{36... | collective-permute-start | bytes 2359304 | tf_op jit(solution)/shard_map/ppermute | solution.py:234
  49.9 14.8 %collective-permute-start.3 = (bf16[3,32,4096]{2,1,0:T(8,128)(2,1)S(1)}, bf16[3,32,4096]{2,1,0:T(8,128)(2,1)S(1)}, u32[]{:S(2)}, u32[]{:S(2)}) collective-permute-start(bf16[3,32,4096]{2,1,0:T(8,128)(2,1)S(1)} %collective-permute-done.1.g1), channel_id=1, source_target_pairs={{0,32},{32,0},{1,33},{33,1},{2,34},{34,2},{3,35},{35,3},{4,36},{36... | collective-permute-start | bytes 2359304 | tf_op jit(solution)/shard_map/ppermute | solution.py:234
  66.9 3.6 %copy-start = (bf16[32,4096]{1,0:T(8,128)(2,1)S(1)}, bf16[32,4096]{1,0:T(8,128)(2,1)}, u32[]{:S(2)}) copy-start(bf16[32,4096]{1,0:T(8,128)(2,1)} %gate_ref.3) | copy-start | bytes 786436
  66.9 3.6 %copy-start.1 = (bf16[32,4096]{1,0:T(8,128)(2,1)S(1)}, bf16[32,4096]{1,0:T(8,128)(2,1)}, u32[]{:S(2)}) copy-start(bf16[32,4096]{1,0:T(8,128)(2,1)} %up_ref.3) | copy-start | bytes 786436
  66.9 20.5 %all-to-all-start.2 = ((bf16[12,96,128]{2,1,0:T(8,128)(2,1)}), bf16[12,96,128]{2,1,0:T(8,128)(2,1)S(1)}, u32[]{:S(2)}, u32[]{:S(2)}) async-start(bf16[12,96,128]{2,1,0:T(8,128)(2,1)} %bitcast.6), calls=%async_computation.2 | async-start | bytes 589824 | tf_op jit(solution)/shard_map/all_to_all | solution.py:266
  70.5 1.0 copy-start.2
  71.4 0.9 copy-start.3

commit v4 on v3

--- a/solution.py
+++ b/solution.py
@@ -94,7 +94,7 @@
 def weights_body(first_ref, gate_ref, up_ref, down_ref, o0, o1, sems):
     copies = []
     for m, out in enumerate((o0, o1)):
-        expert = (first_ref[0] + m) % 2
+        expert = (first_ref[0] + 1 - m) % 2
         for w, ref in enumerate((gate_ref, up_ref, down_ref)):
             copies.append(pltpu.make_async_copy(ref.at[expert], out.at[w], sems.at[m, w]))
             copies[-1].start()
@@ -106,11 +106,20 @@
     return v / (1.0 + jnp.exp(-v))
 
 
-def shared_body(own_ref, gate_ref, up_ref, down_ref, out_ref):
-    own = own_ref[...]
+def shared_body(own_ref, gate_ref, up_ref, down_ref, out_ref, own, gate, up, down, part, sems):
+    pairs = ((own_ref, own), (gate_ref, gate), (up_ref, up), (down_ref, down))
+    copies = [pltpu.make_async_copy(a, b, sems.at[i]) for i, (a, b) in enumerate(pairs)]
+    for copy in copies:
+        copy.start()
+    for copy in copies:
+        copy.wait()
     nt = ((1,), (1,))
-    inner = (silu(dot(own, gate_ref[...], nt)) * dot(own, up_ref[...], nt)).astype(bf16)
-    out_ref[...] = dot(inner, down_ref[...], ((1,), (0,)))
+    x = own[...]
+    inner = (silu(dot(x, gate[...], nt)) * dot(x, up[...], nt)).astype(bf16)
+    part[...] = dot(inner, down[...], ((1,), (0,)))
+    copy = pltpu.make_async_copy(part, out_ref, sems.at[4])
+    copy.start()
+    copy.wait()
 
 
 def experts_body(rows_ref, g0, g1, g2, g3, out_ref, flat):
@@ -228,7 +237,7 @@
         for c in range(N_C):
             for j in range(N_TP):
                 sy, sx = j // N_X, j % N_X
-                target = (sy % 2) * N_TP + (sy - sy % 2 + c) * N_X + (sx - sx % 2 + (sx + m) % 2)
+                target = (sy % 2) * N_TP + (sy - sy % 2 + c) * N_X + (sx - sx % 2 + (sx + 1 - m) % 2)
                 pairs.append((c * N_TP + j, target))
         mine.append(lax.ppermute(piece, ("c", "y", "x"), pairs))
         other.append(lax.ppermute(mine[-1], "c", [(0, 1), (1, 0)]))
@@ -246,12 +255,16 @@
     arrived = lax.all_to_all(packed.reshape(N_Z, CAP * N_TP, LANES), "z", 0, 0, tiled=True)
     shared = call(
         shared_body,
-        [VMEM] * 4,
-        shape((TOK, N_TP * LANES), f32),
+        [ANY] * 4,
+        pltpu.HBM((TOK, N_TP * LANES), f32),
         own,
         shared_gate,
         shared_up,
         shared_down,
+        scratch=[pltpu.VMEM((TOK, N_TP * LANES), bf16)]
+        + [pltpu.VMEM((UNITS, N_TP * LANES), bf16)] * 3
+        + [pltpu.VMEM((TOK, N_TP * LANES), f32), pltpu.SemaphoreType.DMA((5,))],
+        outspecs=[ANY],
     )
     parts = call(
         experts_body,

time: 104 us -> 105 us (level)
  Pallas kernels: 8.46 us -> 10.4 us
    pallas_call x8, Pallas kernels: 8.46 us -> 10.4 us  [call(): pl.pallas_call(body, in_specs=ins, out_specs=outspecs or [VMEM] * len(sha...]
    unnamed x16 -> x10, local copies, waits for them, and re-layouts: 2.58 us -> 1.67 us
  transfers between devices with their start and end apart: 7 -> 7, of which waited for: 3 -> 3; matrix products, arithmetic and copies ran while one was open for 0% -> 0% of each run, Pallas kernels for 4% -> 5%
where the time goes in v4:
time: 105 us
  waiting for transfers between devices  38.9 us (37%)
  starting transfers between devices  38.7 us (37%)
  blocking collectives  14.8 us (14%)
  Pallas kernels  10.4 us (10%)
  local copies, waits for them, and re-layouts  1.67 us (2%)
    all_to_all x1, blocking collectives, per_device(): mixed = lax.all_to_all(mixed, ('y', 'x'), 0, 0, tiled=True)  14.8 us
    all_to_all x1, starting transfers between devices, per_device(): lax.all_to_all(packed.reshape(N_Z, CAP * N_TP, LANES), 'z', 0, 0, tiled=T...  14.8 us
    all_to_all x1, waiting for transfers between devices, per_device(): lax.all_to_all(parts.reshape(N_Z, CAP * N_TP, LANES), 'z', 0, 0, tiled=True)  14.5 us
    all_to_all x1, waiting for transfers between devices, per_device(): lax.all_to_all(packed.reshape(N_Z, CAP * N_TP, LANES), 'z', 0, 0, tiled=T...  12.9 us
    all_to_all x1, waiting for transfers between devices, per_device(): tokens = lax.all_to_all(copies, ('y', 'x'), 0, 0, tiled=True)  11.5 us
    all_to_all x1, starting transfers between devices, per_device(): tokens = lax.all_to_all(copies, ('y', 'x'), 0, 0, tiled=True)  11.3 us
    pallas_call x8, Pallas kernels, call(): pl.pallas_call(body, in_specs=ins, out_specs=outspecs or [VMEM] * len(sha...  10.4 us
    ppermute x2, starting transfers between devices, per_device(): other.append(lax.ppermute(mine[-1], 'c', [(0, 1), (1, 0)]))  5.09 us
  transfers between devices with their start and end apart: 7, of which 3 were waited for; matrix products, arithmetic and copies ran while one was open for 0% of the time, Pallas kernels for 5%

profile of v4, /device:TPU:64, one launch (start us, length us, event | category | flops | bytes accessed | tf_op | source)
XLA Modules:
  0.0 104.7 jit_solution(14952831650360754409)
XLA Ops:
  0.0 1.4 %shard_map.103 = (bf16[3,32,4096]{2,1,0:T(8,128)(2,1)S(1)}, bf16[3,32,4096]{2,1,0:T(8,128)(2,1)S(1)}) custom-call(s32[1]{0:T(128)} %bitcast.5.first_ref, bf16[2,32,4096]{2,1,0:T(8,128)(2,1)} %gate_ref.2, bf16[2,32,4096]{2,1,0:T(8,128)(2,1)} %up_ref.2, bf16[2,32,4096]{2,1,0:T(8,128)(2,1)} %down_ref.2), custom_call_target="tpu_custom_call" | custom-call | tf_op jit(solution)/shard_map/pallas_call | solution.py:177
  1.4 3.4 %collective-permute-start = (bf16[3,32,4096]{2,1,0:T(8,128)(2,1)S(1)}, bf16[3,32,4096]{2,1,0:T(8,128)(2,1)S(1)}, u32[]{:S(2)}, u32[]{:S(2)}) collective-permute-start(bf16[3,32,4096]{2,1,0:T(8,128)(2,1)S(1)} %get-tuple-element.15), channel_id=1, source_target_pairs={{0,1},{1,0},{2,3},{3,2},{4,33},{5,32},{6,35},{7,34},{8,9},{9,8},{1... | collective-permute-start | bytes 2359304 | tf_op jit(solution)/shard_map/ppermute | solution.py:242
  4.8 0.7 collective-permute-start.1
  5.5 1.4 %shard_map.100 = bf16[32,16,128]{2,1,0:T(8,128)(2,1)} custom-call(bf16[16,128]{1,0:T(8,128)(2,1)} %hidden_ref.1), custom_call_target="tpu_custom_call" | custom-call | tf_op jit(solution)/shard_map/pallas_call | solution.py:177
  6.9 0.0 copy-start.2
  6.9 11.3 %all-to-all-start = ((bf16[32,16,128]{2,1,0:T(8,128)(2,1)}), bf16[32,16,128]{2,1,0:T(8,128)(2,1)S(1)}, u32[]{:S(2)}, u32[]{:S(2)}) async-start(bf16[32,16,128]{2,1,0:T(8,128)(2,1)} %shard_map.100), calls=%async_computation | async-start | bytes 262144 | tf_op jit(solution)/shard_map/all_to_all | solution.py:213
  18.2 0.1 copy.11.routes_ref
  18.3 0.1 copy.12.weights_ref
  18.4 0.5 copy-done.1
  18.9 0.2 shard_map.101
  19.1 11.5 %all-to-all-done.rows_ref = bf16[32,16,128]{2,1,0:T(8,128)(2,1)S(1)} async-done(((bf16[32,16,128]{2,1,0:T(8,128)(2,1)}), bf16[32,16,128]{2,1,0:T(8,128)(2,1)S(1)}, u32[]{:S(2)}, u32[]{:S(2)}) %all-to-all-start) | async-done | bytes 131104 | tf_op jit(solution)/shard_map/all_to_all | solution.py:213
  30.6 1.8 %shard_map.102 = (bf16[16,4096]{1,0:T(8,128)(2,1)}, bf16[1152,128]{1,0:T(8,128)(2,1)}) custom-call(bf16[32,16,128]{2,1,0:T(8,128)(2,1)S(1)} %all-to-all-done.rows_ref, f32[32,128]{1,0:T(8,128)S(1)} %get-tuple-element.12.gain_ref, bf16[40,16]{1,0:T(8,128)(2,1)S(1)} %get-tuple-element.13.select_ref), custom_call_target="tpu_custom_call" | custom-call | tf_op jit(solution)/shard_map/pallas_call | solution.py:177
  32.4 14.8 %all-to-all-start.1 = ((bf16[12,96,128]{2,1,0:T(8,128)(2,1)}), bf16[12,96,128]{2,1,0:T(8,128)(2,1)S(1)}, u32[]{:S(2)}, u32[]{:S(2)}) async-start(bf16[12,96,128]{2,1,0:T(8,128)(2,1)} %bitcast.3), calls=%async_computation.1 | async-start | bytes 589824 | tf_op jit(solution)/shard_map/all_to_all | solution.py:255
  47.2 3.2 %collective-permute-start.2 = (bf16[3,32,4096]{2,1,0:T(8,128)(2,1)S(1)}, bf16[3,32,4096]{2,1,0:T(8,128)(2,1)S(1)}, u32[]{:S(2)}, u32[]{:S(2)}) collective-permute-start(bf16[3,32,4096]{2,1,0:T(8,128)(2,1)S(1)} %collective-permute-done.g0), channel_id=1, source_target_pairs={{0,32},{32,0},{1,33},{33,1},{2,34},{34,2},{3,35},{35,3},{4,36},{36... | collective-permute-start | bytes 2359304 | tf_op jit(solution)/shard_map/ppermute | solution.py:243
  50.4 1.9 %collective-permute-start.3 = (bf16[3,32,4096]{2,1,0:T(8,128)(2,1)S(1)}, bf16[3,32,4096]{2,1,0:T(8,128)(2,1)S(1)}, u32[]{:S(2)}, u32[]{:S(2)}) collective-permute-start(bf16[3,32,4096]{2,1,0:T(8,128)(2,1)S(1)} %collective-permute-done.1.g1), channel_id=1, source_target_pairs={{0,32},{32,0},{1,33},{33,1},{2,34},{34,2},{3,35},{35,3},{4,36},{36... | collective-permute-start | bytes 2359304 | tf_op jit(solution)/shard_map/ppermute | solution.py:243
  52.3 12.9 %all-to-all-done.1 = bf16[12,96,128]{2,1,0:T(8,128)(2,1)S(1)} async-done(((bf16[12,96,128]{2,1,0:T(8,128)(2,1)}), bf16[12,96,128]{2,1,0:T(8,128)(2,1)S(1)}, u32[]{:S(2)}, u32[]{:S(2)}) %all-to-all-start.1) | async-done | bytes 294944 | tf_op jit(solution)/shard_map/all_to_all | solution.py:255
  65.2 2.2 %shard_map.104 = bf16[1152,128]{1,0:T(8,128)(2,1)} custom-call(bf16[1152,128]{1,0:T(8,128)(2,1)S(1)} %bitcast.8, bf16[3,32,4096]{2,1,0:T(8,128)(2,1)S(1)} %collective-permute-done.g0, bf16[3,32,4096]{2,1,0:T(8,128)(2,1)S(1)} %collective-permute-done.1.g1, bf16[3,32,4096]{2,1,0:T(8,128)(2,1)S(1)} %collective-permute-done.2.g2, ...), custom_call_target="tpu_custom_call" | custom-call | tf_op jit(solution)/shard_map/pallas_call | solution.py:177
  67.4 3.5 %all-to-all-start.2 = ((bf16[12,96,128]{2,1,0:T(8,128)(2,1)}), bf16[12,96,128]{2,1,0:T(8,128)(2,1)S(1)}, u32[]{:S(2)}, u32[]{:S(2)}) async-start(bf16[12,96,128]{2,1,0:T(8,128)(2,1)} %bitcast.6), calls=%async_computation.2 | async-start | bytes 589824 | tf_op jit(solution)/shard_map/all_to_all | solution.py:279
  70.9 2.3 %shard_map.105.shared_ref = f32[16,4096]{1,0:T(8,128)} custom-call(bf16[16,4096]{1,0:T(8,128)(2,1)} %get-tuple-element.18.own_ref, bf16[32,4096]{1,0:T(8,128)(2,1)} %gate_ref.3, bf16[32,4096]{1,0:T(8,128)(2,1)} %up_ref.3, bf16[32,4096]{1,0:T(8,128)(2,1)} %down_ref.3), custom_call_target="tpu_custom_call" | custom-call | tf_op jit(solution)/shard_map/pallas_call | solution.py:177
  73.2 14.5 %all-to-all-done.2 = bf16[12,96,128]{2,1,0:T(8,128)(2,1)S(1)} async-done(((bf16[12,96,128]{2,1,0:T(8,128)(2,1)}), bf16[12,96,128]{2,1,0:T(8,128)(2,1)S(1)}, u32[]{:S(2)}, u32[]{:S(2)}) %all-to-all-start.2) | async-done | bytes 294944 | tf_op jit(solution)/shard_map/all_to_all | solution.py:279
  87.7 0.9 copy-done
  88.7 0.5 shard_map.106
  89.2 14.8 %all_to_all.20.parts_ref = bf16[32,16,128]{2,1,0:T(8,128)(2,1)S(1)} all-to-all(bf16[32,16,128]{2,1,0:T(8,128)(2,1)S(1)} %shard_map.106), channel_id=1, replica_groups=mesh['z'=12,'c'=2,'y'=8,'x'=4] {'y','x'}, dimensions={0} | all-to-all | bytes 262144 | tf_op jit(solution)/shard_map/all_to_all | solution.py:289
  104.1 0.6 shard_map.107
  (9 shorter events, 0.0 us)
Async XLA Ops:
  1.4 45.8 %collective-permute-start = (bf16[3,32,4096]{2,1,0:T(8,128)(2,1)S(1)}, bf16[3,32,4096]{2,1,0:T(8,128)(2,1)S(1)}, u32[]{:S(2)}, u32[]{:S(2)}) collective-permute-start(bf16[3,32,4096]{2,1,0:T(8,128)(2,1)S(1)} %get-tuple-element.15), channel_id=1, source_target_pairs={{0,1},{1,0},{2,3},{3,2},{4,33},{5,32},{6,35},{7,34},{8,9},{9,8},{1... | collective-permute-start | bytes 2359304 | tf_op jit(solution)/shard_map/ppermute | solution.py:242
  4.8 45.6 %collective-permute-start.1 = (bf16[3,32,4096]{2,1,0:T(8,128)(2,1)S(1)}, bf16[3,32,4096]{2,1,0:T(8,128)(2,1)S(1)}, u32[]{:S(2)}, u32[]{:S(2)}) collective-permute-start(bf16[3,32,4096]{2,1,0:T(8,128)(2,1)S(1)} %get-tuple-element.16), channel_id=1, source_target_pairs={{0,0},{1,1},{2,2},{3,3},{4,32},{5,33},{6,34},{7,35},{8,8},{9,9},{1... | collective-permute-start | bytes 2359304 | tf_op jit(solution)/shard_map/ppermute | solution.py:242
  6.9 11.3 %copy-start.2 = (s32[16,4]{0,1:T(4,128)S(1)}, s32[16,4]{0,1:T(4,128)}, u32[]{:S(2)}) copy-start(s32[16,4]{0,1:T(4,128)} %param.12) | copy-start | bytes 772
  6.9 11.4 %copy-start.3 = (f32[16,4]{0,1:T(4,128)S(1)}, f32[16,4]{0,1:T(4,128)}, u32[]{:S(2)}) copy-start(f32[16,4]{0,1:T(4,128)} %param.13) | copy-start | bytes 772
  6.9 23.7 %all-to-all-start = ((bf16[32,16,128]{2,1,0:T(8,128)(2,1)}), bf16[32,16,128]{2,1,0:T(8,128)(2,1)S(1)}, u32[]{:S(2)}, u32[]{:S(2)}) async-start(bf16[32,16,128]{2,1,0:T(8,128)(2,1)} %shard_map.100), calls=%async_computation | async-start | bytes 262144 | tf_op jit(solution)/shard_map/all_to_all | solution.py:213
  18.2 0.7 copy-start.1
  32.4 32.8 %all-to-all-start.1 = ((bf16[12,96,128]{2,1,0:T(8,128)(2,1)}), bf16[12,96,128]{2,1,0:T(8,128)(2,1)S(1)}, u32[]{:S(2)}, u32[]{:S(2)}) async-start(bf16[12,96,128]{2,1,0:T(8,128)(2,1)} %bitcast.3), calls=%async_computation.1 | async-start | bytes 589824 | tf_op jit(solution)/shard_map/all_to_all | solution.py:255
  47.2 18.0 %collective-permute-start.2 = (bf16[3,32,4096]{2,1,0:T(8,128)(2,1)S(1)}, bf16[3,32,4096]{2,1,0:T(8,128)(2,1)S(1)}, u32[]{:S(2)}, u32[]{:S(2)}) collective-permute-start(bf16[3,32,4096]{2,1,0:T(8,128)(2,1)S(1)} %collective-permute-done.g0), channel_id=1, source_target_pairs={{0,32},{32,0},{1,33},{33,1},{2,34},{34,2},{3,35},{35,3},{4,36},{36... | collective-permute-start | bytes 2359304 | tf_op jit(solution)/shard_map/ppermute | solution.py:243
  50.4 14.8 %collective-permute-start.3 = (bf16[3,32,4096]{2,1,0:T(8,128)(2,1)S(1)}, bf16[3,32,4096]{2,1,0:T(8,128)(2,1)S(1)}, u32[]{:S(2)}, u32[]{:S(2)}) collective-permute-start(bf16[3,32,4096]{2,1,0:T(8,128)(2,1)S(1)} %collective-permute-done.1.g1), channel_id=1, source_target_pairs={{0,32},{32,0},{1,33},{33,1},{2,34},{34,2},{3,35},{35,3},{4,36},{36... | collective-permute-start | bytes 2359304 | tf_op jit(solution)/shard_map/ppermute | solution.py:243
  67.4 20.3 %all-to-all-start.2 = ((bf16[12,96,128]{2,1,0:T(8,128)(2,1)}), bf16[12,96,128]{2,1,0:T(8,128)(2,1)S(1)}, u32[]{:S(2)}, u32[]{:S(2)}) async-start(bf16[12,96,128]{2,1,0:T(8,128)(2,1)} %bitcast.6), calls=%async_computation.2 | async-start | bytes 589824 | tf_op jit(solution)/shard_map/all_to_all | solution.py:279
  87.7 1.0 copy-start

commit v5 on v4

--- a/solution.py
+++ b/solution.py
@@ -71,24 +71,28 @@
         left = left - term.astype(f32)
 
 
-def norm_body(rows_ref, gain_ref, select_ref, own_ref, out_ref, flat, kept, sem):
-    squares = jnp.zeros((TOK, LANES), f32)
+def norm_body(rows_ref, gain_ref, select_ref, own_ref, out_ref, flat, kept, packed, sems):
+    squares = [jnp.zeros((TOK, LANES), f32)] * 4
     for s in range(N_TP):
         v = rows_ref[s].astype(f32)
-        squares = squares + v * v
-    inv = lax.rsqrt(jnp.sum(squares, axis=1, keepdims=True) * (1.0 / (N_TP * LANES)) + norm_eps)
+        squares[s % 4] = squares[s % 4] + v * v
+    total = jnp.sum((squares[0] + squares[1]) + (squares[2] + squares[3]), axis=1, keepdims=True)
+    inv = lax.rsqrt(total * (1.0 / (N_TP * LANES)) + norm_eps)
     for s in range(N_TP):
         kept[:, s * LANES : (s + 1) * LANES] = (
             rows_ref[s].astype(f32) * inv * gain_ref[s : s + 1, :]
         ).astype(bf16)
-    copy = pltpu.make_async_copy(kept, own_ref, sem)
-    copy.start()
+    own_copy = pltpu.make_async_copy(kept, own_ref, sems.at[0])
+    own_copy.start()
     select = select_ref[...]
     for s in range(N_TP):
         piece = kept[:, s * LANES : (s + 1) * LANES]
         flat[pl.ds(s, ROWS, stride=N_TP), :] = dot(select, piece, ((1,), (0,)))[0:ROWS]
-    out_ref[...] = flat[...].astype(bf16)
-    copy.wait()
+    packed[...] = flat[...].astype(bf16)
+    out_copy = pltpu.make_async_copy(packed, out_ref, sems.at[1])
+    out_copy.start()
+    own_copy.wait()
+    out_copy.wait()
 
 
 def weights_body(first_ref, gate_ref, up_ref, down_ref, o0, o1, sems):
@@ -245,12 +249,17 @@
     own, packed = call(
         norm_body,
         [VMEM] * 3,
-        [pltpu.HBM((TOK, N_TP * LANES), bf16), shape((ROWS * N_TP, LANES))],
+        [pltpu.HBM((TOK, N_TP * LANES), bf16), pltpu.HBM((ROWS * N_TP, LANES), bf16)],
         tokens,
         gain,
         select,
-        scratch=[flat, pltpu.VMEM((TOK, N_TP * LANES), bf16), pltpu.SemaphoreType.DMA],
-        outspecs=[ANY, VMEM],
+        scratch=[
+            flat,
+            pltpu.VMEM((TOK, N_TP * LANES), bf16),
+            pltpu.VMEM((ROWS * N_TP, LANES), bf16),
+            pltpu.SemaphoreType.DMA((2,)),
+        ],
+        outspecs=[ANY, ANY],
     )
     arrived = lax.all_to_all(packed.reshape(N_Z, CAP * N_TP, LANES), "z", 0, 0, tiled=True)
     shared = call(

time: 105 us -> 105 us (level)
  no operation moved by 1% of the time
where the time goes in v5:
time: 105 us; the launch traced here: 104 us
  waiting for transfers between devices  38.9 us (37%)
  starting transfers between devices  38.7 us (37%)
  blocking collectives  14.8 us (14%)
  Pallas kernels  10.1 us (10%)
  local copies, waits for them, and re-layouts  1.67 us (2%)
    all_to_all x1, blocking collectives, per_device(): mixed = lax.all_to_all(mixed, ('y', 'x'), 0, 0, tiled=True)  14.8 us
    all_to_all x1, starting transfers between devices, per_device(): lax.all_to_all(packed.reshape(N_Z, CAP * N_TP, LANES), 'z', 0, 0, tiled=T...  14.8 us
    all_to_all x1, waiting for transfers between devices, per_device(): lax.all_to_all(parts.reshape(N_Z, CAP * N_TP, LANES), 'z', 0, 0, tiled=True)  14.5 us
    all_to_all x1, waiting for transfers between devices, per_device(): lax.all_to_all(packed.reshape(N_Z, CAP * N_TP, LANES), 'z', 0, 0, tiled=T...  12.9 us
    all_to_all x1, waiting for transfers between devices, per_device(): tokens = lax.all_to_all(copies, ('y', 'x'), 0, 0, tiled=True)  11.5 us
    all_to_all x1, starting transfers between devices, per_device(): tokens = lax.all_to_all(copies, ('y', 'x'), 0, 0, tiled=True)  11.3 us
    pallas_call x8, Pallas kernels, call(): pl.pallas_call(body, in_specs=ins, out_specs=outspecs or [VMEM] * len(sha...  10.1 us
    ppermute x2, starting transfers between devices, per_device(): other.append(lax.ppermute(mine[-1], 'c', [(0, 1), (1, 0)]))  5.09 us
  transfers between devices with their start and end apart: 7, of which 3 were waited for; matrix products, arithmetic and copies ran while one was open for 0% of the time, Pallas kernels for 5%

profile of v5, /device:TPU:64, one launch (start us, length us, event | category | flops | bytes accessed | tf_op | source)
XLA Modules:
  0.0 104.4 jit_solution(2764688038693444652)
XLA Ops:
  0.0 1.4 %shard_map.103 = (bf16[3,32,4096]{2,1,0:T(8,128)(2,1)S(1)}, bf16[3,32,4096]{2,1,0:T(8,128)(2,1)S(1)}) custom-call(s32[1]{0:T(128)} %bitcast.5.first_ref, bf16[2,32,4096]{2,1,0:T(8,128)(2,1)} %gate_ref.2, bf16[2,32,4096]{2,1,0:T(8,128)(2,1)} %up_ref.2, bf16[2,32,4096]{2,1,0:T(8,128)(2,1)} %down_ref.2), custom_call_target="tpu_custom_call" | custom-call | tf_op jit(solution)/shard_map/pallas_call | solution.py:181
  1.4 3.4 %collective-permute-start = (bf16[3,32,4096]{2,1,0:T(8,128)(2,1)S(1)}, bf16[3,32,4096]{2,1,0:T(8,128)(2,1)S(1)}, u32[]{:S(2)}, u32[]{:S(2)}) collective-permute-start(bf16[3,32,4096]{2,1,0:T(8,128)(2,1)S(1)} %get-tuple-element.15), channel_id=1, source_target_pairs={{0,1},{1,0},{2,3},{3,2},{4,33},{5,32},{6,35},{7,34},{8,9},{9,8},{1... | collective-permute-start | bytes 2359304 | tf_op jit(solution)/shard_map/ppermute | solution.py:246
  4.8 0.7 collective-permute-start.1
  5.5 1.4 %shard_map.100 = bf16[32,16,128]{2,1,0:T(8,128)(2,1)} custom-call(bf16[16,128]{1,0:T(8,128)(2,1)} %hidden_ref.1), custom_call_target="tpu_custom_call" | custom-call | tf_op jit(solution)/shard_map/pallas_call | solution.py:181
  6.9 0.0 copy-start.2
  6.9 11.3 %all-to-all-start = ((bf16[32,16,128]{2,1,0:T(8,128)(2,1)}), bf16[32,16,128]{2,1,0:T(8,128)(2,1)S(1)}, u32[]{:S(2)}, u32[]{:S(2)}) async-start(bf16[32,16,128]{2,1,0:T(8,128)(2,1)} %shard_map.100), calls=%async_computation | async-start | bytes 262144 | tf_op jit(solution)/shard_map/all_to_all | solution.py:217
  18.2 0.1 copy.11.routes_ref
  18.3 0.1 copy.12.weights_ref
  18.4 0.5 copy-done.1
  18.9 0.2 shard_map.101
  19.1 11.5 %all-to-all-done.rows_ref = bf16[32,16,128]{2,1,0:T(8,128)(2,1)S(1)} async-done(((bf16[32,16,128]{2,1,0:T(8,128)(2,1)}), bf16[32,16,128]{2,1,0:T(8,128)(2,1)S(1)}, u32[]{:S(2)}, u32[]{:S(2)}) %all-to-all-start) | async-done | bytes 131104 | tf_op jit(solution)/shard_map/all_to_all | solution.py:217
  30.6 1.4 %shard_map.102 = (bf16[16,4096]{1,0:T(8,128)(2,1)}, bf16[1152,128]{1,0:T(8,128)(2,1)}) custom-call(bf16[32,16,128]{2,1,0:T(8,128)(2,1)S(1)} %all-to-all-done.rows_ref, f32[32,128]{1,0:T(8,128)S(1)} %get-tuple-element.12.gain_ref, bf16[40,16]{1,0:T(8,128)(2,1)S(1)} %get-tuple-element.13.select_ref), custom_call_target="tpu_custom_call" | custom-call | tf_op jit(solution)/shard_map/pallas_call | solution.py:181
  32.1 14.8 %all-to-all-start.1 = ((bf16[12,96,128]{2,1,0:T(8,128)(2,1)}), bf16[12,96,128]{2,1,0:T(8,128)(2,1)S(1)}, u32[]{:S(2)}, u32[]{:S(2)}) async-start(bf16[12,96,128]{2,1,0:T(8,128)(2,1)} %bitcast.12), calls=%async_computation.1 | async-start | bytes 589824 | tf_op jit(solution)/shard_map/all_to_all | solution.py:264
  46.9 3.2 %collective-permute-start.2 = (bf16[3,32,4096]{2,1,0:T(8,128)(2,1)S(1)}, bf16[3,32,4096]{2,1,0:T(8,128)(2,1)S(1)}, u32[]{:S(2)}, u32[]{:S(2)}) collective-permute-start(bf16[3,32,4096]{2,1,0:T(8,128)(2,1)S(1)} %collective-permute-done.g0), channel_id=1, source_target_pairs={{0,32},{32,0},{1,33},{33,1},{2,34},{34,2},{3,35},{35,3},{4,36},{36... | collective-permute-start | bytes 2359304 | tf_op jit(solution)/shard_map/ppermute | solution.py:247
  50.1 1.9 %collective-permute-start.3 = (bf16[3,32,4096]{2,1,0:T(8,128)(2,1)S(1)}, bf16[3,32,4096]{2,1,0:T(8,128)(2,1)S(1)}, u32[]{:S(2)}, u32[]{:S(2)}) collective-permute-start(bf16[3,32,4096]{2,1,0:T(8,128)(2,1)S(1)} %collective-permute-done.1.g1), channel_id=1, source_target_pairs={{0,32},{32,0},{1,33},{33,1},{2,34},{34,2},{3,35},{35,3},{4,36},{36... | collective-permute-start | bytes 2359304 | tf_op jit(solution)/shard_map/ppermute | solution.py:247
  52.0 12.9 %all-to-all-done.1 = bf16[12,96,128]{2,1,0:T(8,128)(2,1)S(1)} async-done(((bf16[12,96,128]{2,1,0:T(8,128)(2,1)}), bf16[12,96,128]{2,1,0:T(8,128)(2,1)S(1)}, u32[]{:S(2)}, u32[]{:S(2)}) %all-to-all-start.1) | async-done | bytes 294944 | tf_op jit(solution)/shard_map/all_to_all | solution.py:264
  64.9 2.2 %shard_map.104 = bf16[1152,128]{1,0:T(8,128)(2,1)} custom-call(bf16[1152,128]{1,0:T(8,128)(2,1)S(1)} %bitcast.8, bf16[3,32,4096]{2,1,0:T(8,128)(2,1)S(1)} %collective-permute-done.g0, bf16[3,32,4096]{2,1,0:T(8,128)(2,1)S(1)} %collective-permute-done.1.g1, bf16[3,32,4096]{2,1,0:T(8,128)(2,1)S(1)} %collective-permute-done.2.g2, ...), custom_call_target="tpu_custom_call" | custom-call | tf_op jit(solution)/shard_map/pallas_call | solution.py:181
  67.1 3.5 %all-to-all-start.2 = ((bf16[12,96,128]{2,1,0:T(8,128)(2,1)}), bf16[12,96,128]{2,1,0:T(8,128)(2,1)S(1)}, u32[]{:S(2)}, u32[]{:S(2)}) async-start(bf16[12,96,128]{2,1,0:T(8,128)(2,1)} %bitcast.6), calls=%async_computation.2 | async-start | bytes 589824 | tf_op jit(solution)/shard_map/all_to_all | solution.py:288
  70.6 2.3 %shard_map.105.shared_ref = f32[16,4096]{1,0:T(8,128)} custom-call(bf16[16,4096]{1,0:T(8,128)(2,1)} %get-tuple-element.18.own_ref, bf16[32,4096]{1,0:T(8,128)(2,1)} %gate_ref.3, bf16[32,4096]{1,0:T(8,128)(2,1)} %up_ref.3, bf16[32,4096]{1,0:T(8,128)(2,1)} %down_ref.3), custom_call_target="tpu_custom_call" | custom-call | tf_op jit(solution)/shard_map/pallas_call | solution.py:181
  72.9 14.5 %all-to-all-done.2 = bf16[12,96,128]{2,1,0:T(8,128)(2,1)S(1)} async-done(((bf16[12,96,128]{2,1,0:T(8,128)(2,1)}), bf16[12,96,128]{2,1,0:T(8,128)(2,1)S(1)}, u32[]{:S(2)}, u32[]{:S(2)}) %all-to-all-start.2) | async-done | bytes 294944 | tf_op jit(solution)/shard_map/all_to_all | solution.py:288
  87.5 0.9 copy-done
  88.4 0.5 shard_map.106
  88.9 14.8 %all_to_all.20.parts_ref = bf16[32,16,128]{2,1,0:T(8,128)(2,1)S(1)} all-to-all(bf16[32,16,128]{2,1,0:T(8,128)(2,1)S(1)} %shard_map.106), channel_id=1, replica_groups=mesh['z'=12,'c'=2,'y'=8,'x'=4] {'y','x'}, dimensions={0} | all-to-all | bytes 262144 | tf_op jit(solution)/shard_map/all_to_all | solution.py:298
  103.8 0.6 shard_map.107
  (9 shorter events, 0.0 us)
Async XLA Ops:
  1.4 45.5 %collective-permute-start = (bf16[3,32,4096]{2,1,0:T(8,128)(2,1)S(1)}, bf16[3,32,4096]{2,1,0:T(8,128)(2,1)S(1)}, u32[]{:S(2)}, u32[]{:S(2)}) collective-permute-start(bf16[3,32,4096]{2,1,0:T(8,128)(2,1)S(1)} %get-tuple-element.15), channel_id=1, source_target_pairs={{0,1},{1,0},{2,3},{3,2},{4,33},{5,32},{6,35},{7,34},{8,9},{9,8},{1... | collective-permute-start | bytes 2359304 | tf_op jit(solution)/shard_map/ppermute | solution.py:246
  4.8 45.3 %collective-permute-start.1 = (bf16[3,32,4096]{2,1,0:T(8,128)(2,1)S(1)}, bf16[3,32,4096]{2,1,0:T(8,128)(2,1)S(1)}, u32[]{:S(2)}, u32[]{:S(2)}) collective-permute-start(bf16[3,32,4096]{2,1,0:T(8,128)(2,1)S(1)} %get-tuple-element.16), channel_id=1, source_target_pairs={{0,0},{1,1},{2,2},{3,3},{4,32},{5,33},{6,34},{7,35},{8,8},{9,9},{1... | collective-permute-start | bytes 2359304 | tf_op jit(solution)/shard_map/ppermute | solution.py:246
  6.9 11.3 %copy-start.2 = (s32[16,4]{0,1:T(4,128)S(1)}, s32[16,4]{0,1:T(4,128)}, u32[]{:S(2)}) copy-start(s32[16,4]{0,1:T(4,128)} %param.12) | copy-start | bytes 772
  6.9 11.4 %copy-start.3 = (f32[16,4]{0,1:T(4,128)S(1)}, f32[16,4]{0,1:T(4,128)}, u32[]{:S(2)}) copy-start(f32[16,4]{0,1:T(4,128)} %param.13) | copy-start | bytes 772
  6.9 23.7 %all-to-all-start = ((bf16[32,16,128]{2,1,0:T(8,128)(2,1)}), bf16[32,16,128]{2,1,0:T(8,128)(2,1)S(1)}, u32[]{:S(2)}, u32[]{:S(2)}) async-start(bf16[32,16,128]{2,1,0:T(8,128)(2,1)} %shard_map.100), calls=%async_computation | async-start | bytes 262144 | tf_op jit(solution)/shard_map/all_to_all | solution.py:217
  18.2 0.7 copy-start.1
  32.1 32.8 %all-to-all-start.1 = ((bf16[12,96,128]{2,1,0:T(8,128)(2,1)}), bf16[12,96,128]{2,1,0:T(8,128)(2,1)S(1)}, u32[]{:S(2)}, u32[]{:S(2)}) async-start(bf16[12,96,128]{2,1,0:T(8,128)(2,1)} %bitcast.12), calls=%async_computation.1 | async-start | bytes 589824 | tf_op jit(solution)/shard_map/all_to_all | solution.py:264
  46.9 18.0 %collective-permute-start.2 = (bf16[3,32,4096]{2,1,0:T(8,128)(2,1)S(1)}, bf16[3,32,4096]{2,1,0:T(8,128)(2,1)S(1)}, u32[]{:S(2)}, u32[]{:S(2)}) collective-permute-start(bf16[3,32,4096]{2,1,0:T(8,128)(2,1)S(1)} %collective-permute-done.g0), channel_id=1, source_target_pairs={{0,32},{32,0},{1,33},{33,1},{2,34},{34,2},{3,35},{35,3},{4,36},{36... | collective-permute-start | bytes 2359304 | tf_op jit(solution)/shard_map/ppermute | solution.py:247
  50.1 14.8 %collective-permute-start.3 = (bf16[3,32,4096]{2,1,0:T(8,128)(2,1)S(1)}, bf16[3,32,4096]{2,1,0:T(8,128)(2,1)S(1)}, u32[]{:S(2)}, u32[]{:S(2)}) collective-permute-start(bf16[3,32,4096]{2,1,0:T(8,128)(2,1)S(1)} %collective-permute-done.1.g1), channel_id=1, source_target_pairs={{0,32},{32,0},{1,33},{33,1},{2,34},{34,2},{3,35},{35,3},{4,36},{36... | collective-permute-start | bytes 2359304 | tf_op jit(solution)/shard_map/ppermute | solution.py:247
  67.1 20.3 %all-to-all-start.2 = ((bf16[12,96,128]{2,1,0:T(8,128)(2,1)}), bf16[12,96,128]{2,1,0:T(8,128)(2,1)S(1)}, u32[]{:S(2)}, u32[]{:S(2)}) async-start(bf16[12,96,128]{2,1,0:T(8,128)(2,1)} %bitcast.6), calls=%async_computation.2 | async-start | bytes 589824 | tf_op jit(solution)/shard_map/all_to_all | solution.py:288
  87.4 1.0 copy-start

commit v6 on v5

--- a/solution.py
+++ b/solution.py
@@ -30,13 +30,27 @@
     return lax.dot_general(a, b, (dims, ((), ())), preferred_element_type=f32, precision=precision)
 
 
-def copies_body(hidden_ref, out_ref, own, sem):
-    copy = pltpu.make_async_copy(hidden_ref, own, sem)
-    copy.start()
-    copy.wait()
+def first_body(bit_ref, hidden_ref, gate_ref, up_ref, down_ref, *refs):
+    small, (copies_ref, o0, o1), kept, (own, wide, sems) = refs[:3], refs[3:6], refs[6:9], refs[9:]
+    own_copy = pltpu.make_async_copy(hidden_ref, own, sems.at[0])
+    own_copy.start()
+    waits = []
+    for i in range(3):
+        waits.append(pltpu.make_async_copy(small[i], kept[i], sems.at[8 + i]))
+        waits[-1].start()
+    for m, out in enumerate((o0, o1)):
+        expert = (bit_ref[0] + 1 - m) % 2
+        for w, ref in enumerate((gate_ref, up_ref, down_ref)):
+            waits.append(pltpu.make_async_copy(ref.at[expert], out.at[w], sems.at[1 + 3 * m + w]))
+            waits[-1].start()
+    own_copy.wait()
     value = own[...]
     for j in range(N_TP):
-        out_ref[j] = value
+        wide[j] = value
+    waits.append(pltpu.make_async_copy(wide, copies_ref, sems.at[7]))
+    waits[-1].start()
+    for copy in waits:
+        copy.wait()
 
 
 def slot_of(shape, dim):
@@ -45,24 +59,29 @@
     return block, (row - CAP * block).astype(f32)
 
 
-def tables_body(place_ref, across_ref, routes_ref, weights_ref, gain_ref, select_ref, combine_ref, kept_ref):
-    kept_ref[...] = gain_ref[...]
+def tables_body(place_ref, across_ref, weights_ref, select_ref, combine_ref):
     place = place_ref[0]
     block, wanted = slot_of((PADDED, TOK), 0)
     named = jnp.zeros((PADDED, TOK), f32)
     for k in range(4):
         named = named + jnp.where(across_ref[k : k + 1, :] == N_Q * block + place, 1.0, 0.0)
-    earlier = jnp.where(iota((TOK, TOK), 0) < iota((TOK, TOK), 1), 1.0, 0.0).astype(bf16)
+    row, column = iota((TOK, TOK), 0), iota((TOK, TOK), 1)
+    earlier = jnp.where(row < column, 1.0, 0.0).astype(bf16)
     rank = dot(named.astype(bf16), earlier, ((1,), (0,)))
     select_ref[...] = jnp.where(rank == wanted, named, 0.0).astype(bf16)
+    same = jnp.where(row == column, 1.0, 0.0)
+    nt = ((1,), (1,))
+    routes = dot(same, across_ref[...].astype(f32), nt, lax.Precision.HIGHEST)
+    weights = dot(same, weights_ref[...], nt, lax.Precision.HIGHEST)
     block, wanted = slot_of((TOK, PADDED), 1)
+    expert = (N_Q * block + place).astype(f32)
     named = jnp.zeros((TOK, PADDED), f32)
     total = jnp.zeros((TOK, PADDED), f32)
     for k in range(4):
-        hit = routes_ref[:, k : k + 1] == N_Q * block + place
+        hit = routes[:, k : k + 1] == expert
         named = named + jnp.where(hit, 1.0, 0.0)
-        total = total + jnp.where(hit, weights_ref[:, k : k + 1], 0.0)
-    earlier = jnp.where(iota((TOK, TOK), 1) < iota((TOK, TOK), 0), 1.0, 0.0).astype(bf16)
+        total = total + jnp.where(hit, weights[:, k : k + 1], 0.0)
+    earlier = jnp.where(column < row, 1.0, 0.0).astype(bf16)
     rank = dot(earlier, named.astype(bf16), ((1,), (0,)))
     left = jnp.where(rank == wanted, total, 0.0)
     for n in range(3):
@@ -93,17 +112,6 @@
     out_copy.start()
     own_copy.wait()
     out_copy.wait()
-
-
-def weights_body(first_ref, gate_ref, up_ref, down_ref, o0, o1, sems):
-    copies = []
-    for m, out in enumerate((o0, o1)):
-        expert = (first_ref[0] + 1 - m) % 2
-        for w, ref in enumerate((gate_ref, up_ref, down_ref)):
-            copies.append(pltpu.make_async_copy(ref.at[expert], out.at[w], sems.at[m, w]))
-            copies[-1].start()
-    for copy in copies:
-        copy.wait()
 
 
 def silu(v):
@@ -207,36 +215,44 @@
 ):
     y, x = lax.axis_index("y"), lax.axis_index("x")
     place = 2 * (y % 2) + x % 2
-    copies = call(
-        copies_body,
-        [ANY],
-        shape((N_TP, TOK, LANES)),
+    piece = shape((3, UNITS, N_TP * LANES))
+    copies, take0, take1, across, weights, gain = call(
+        first_body,
+        [SMEM] + [ANY] * 7,
+        [
+            pltpu.HBM((N_TP, TOK, LANES), bf16),
+            piece,
+            piece,
+            shape(routes.shape[::-1], jnp.int32),
+            shape(routes.shape[::-1], f32),
+            shape((N_TP, LANES), f32),
+        ],
+        (x % 2).reshape(1).astype(jnp.int32),
         hidden,
-        scratch=[pltpu.VMEM((TOK, LANES), bf16), pltpu.SemaphoreType.DMA],
-    )
-    tokens = lax.all_to_all(copies, ("y", "x"), 0, 0, tiled=True)
-    select, combine, gain = call(
-        tables_body,
-        [SMEM] + [VMEM] * 4,
-        [shape((PADDED, TOK)), shape((3 * TOK, PADDED)), shape((N_TP, LANES), f32)],
-        place.reshape(1).astype(jnp.int32),
-        routes.T,
-        routes,
-        route_weights,
-        norm_gain.reshape(N_TP, LANES),
-    )
-    pieces = call(
-        weights_body,
-        [SMEM, ANY, ANY, ANY],
-        [shape((3, UNITS, N_TP * LANES))] * 2,
-        (place % 2).reshape(1).astype(jnp.int32),
         gate_weight,
         up_weight,
         down_weight,
-        scratch=[pltpu.SemaphoreType.DMA((2, 3))],
+        routes.T,
+        route_weights.T,
+        norm_gain.reshape(N_TP, LANES),
+        scratch=[
+            pltpu.VMEM((TOK, LANES), bf16),
+            pltpu.VMEM((N_TP, TOK, LANES), bf16),
+            pltpu.SemaphoreType.DMA((11,)),
+        ],
+        outspecs=[ANY] + [VMEM] * 5,
+    )
+    tokens = lax.all_to_all(copies, ("y", "x"), 0, 0, tiled=True)
+    select, combine = call(
+        tables_body,
+        [SMEM] + [VMEM] * 2,
+        [shape((PADDED, TOK)), shape((3 * TOK, PADDED))],
+        place.reshape(1).astype(jnp.int32),
+        across,
+        weights,
     )
     mine, other = [], []
-    for m, piece in enumerate(pieces):
+    for m, piece in enumerate((take0, take1)):
         pairs = []
         for c in range(N_C):
             for j in range(N_TP):

time: 105 us -> 105 us (level)
  waiting for transfers between devices: 38.9 us -> 40.8 us
  Pallas kernels: 10.1 us -> 9.02 us
    all_to_all x1, waiting for transfers between devices: 11.5 us -> 13.5 us  [per_device(): tokens = lax.all_to_all(copies, ('y', 'x'), 0, 0, tiled=True)]
    pallas_call x8 -> x7, Pallas kernels: 10.1 us -> 9.02 us  [call(): pl.pallas_call(body, in_specs=ins, out_specs=outspecs or [VMEM] * len(sha...]
  transfers between devices with their start and end apart: 7 -> 7, of which waited for: 3 -> 3; matrix products, arithmetic and copies ran while one was open for 0% -> 0% of each run, Pallas kernels for 5% -> 4%
where the time goes in v6:
time: 105 us; the launch traced here: 104 us
  waiting for transfers between devices  40.8 us (39%)
  starting transfers between devices  38.7 us (37%)
  blocking collectives  14.8 us (14%)
  Pallas kernels  9.02 us (9%)
    all_to_all x1, blocking collectives, per_device(): mixed = lax.all_to_all(mixed, ('y', 'x'), 0, 0, tiled=True)  14.8 us
    all_to_all x1, starting transfers between devices, per_device(): lax.all_to_all(packed.reshape(N_Z, CAP * N_TP, LANES), 'z', 0, 0, tiled=T...  14.8 us
    all_to_all x1, waiting for transfers between devices, per_device(): lax.all_to_all(parts.reshape(N_Z, CAP * N_TP, LANES), 'z', 0, 0, tiled=True)  14.5 us
    all_to_all x1, waiting for transfers between devices, per_device(): tokens = lax.all_to_all(copies, ('y', 'x'), 0, 0, tiled=True)  13.5 us
    all_to_all x1, waiting for transfers between devices, per_device(): lax.all_to_all(packed.reshape(N_Z, CAP * N_TP, LANES), 'z', 0, 0, tiled=T...  12.9 us
    all_to_all x1, starting transfers between devices, per_device(): tokens = lax.all_to_all(copies, ('y', 'x'), 0, 0, tiled=True)  11.3 us
    pallas_call x7, Pallas kernels, call(): pl.pallas_call(body, in_specs=ins, out_specs=outspecs or [VMEM] * len(sha...  9.02 us
    ppermute x2, starting transfers between devices, per_device(): other.append(lax.ppermute(mine[-1], 'c', [(0, 1), (1, 0)]))  5.1 us
  transfers between devices with their start and end apart: 7, of which 3 were waited for; matrix products, arithmetic and copies ran while one was open for 0% of the time, Pallas kernels for 4%

profile of v6, /device:TPU:64, one launch (start us, length us, event | category | flops | bytes accessed | tf_op | source)
XLA Modules:
  0.0 104.5 jit_solution(16519570582359703454)
XLA Ops:
  0.0 1.5 %shard_map.100 = (bf16[32,16,128]{2,1,0:T(8,128)(2,1)}, bf16[3,32,4096]{2,1,0:T(8,128)(2,1)S(1)}, bf16[3,32,4096]{2,1,0:T(8,128)(2,1)S(1)}, s32[4,16]{1,0:T(4,12...) custom-call(s32[1]{0:T(128)} %bitcast.bit_ref, bf16[16,128]{1,0:T(8,128)(2,1)} %hidden_ref.1, ...), custom_call_target="tpu_custom_call" | custom-call | tf_op jit(solution)/shard_map/pallas_call | solution.py:189
  1.5 3.4 %collective-permute-start = (bf16[3,32,4096]{2,1,0:T(8,128)(2,1)S(1)}, bf16[3,32,4096]{2,1,0:T(8,128)(2,1)S(1)}, u32[]{:S(2)}, u32[]{:S(2)}) collective-permute-start(bf16[3,32,4096]{2,1,0:T(8,128)(2,1)S(1)} %get-tuple-element.21), channel_id=1, source_target_pairs={{0,1},{1,0},{2,3},{3,2},{4,33},{5,32},{6,35},{7,34},{8,9},{9,8},{1... | collective-permute-start | bytes 2359304 | tf_op jit(solution)/shard_map/ppermute | solution.py:262
  4.9 0.7 collective-permute-start.1
  5.6 11.3 %all-to-all-start = ((bf16[32,16,128]{2,1,0:T(8,128)(2,1)}), bf16[32,16,128]{2,1,0:T(8,128)(2,1)S(1)}, u32[]{:S(2)}, u32[]{:S(2)}) async-start(bf16[32,16,128]{2,1,0:T(8,128)(2,1)} %get-tuple-element.15), calls=%async_computation | async-start | bytes 262144 | tf_op jit(solution)/shard_map/all_to_all | solution.py:245
  16.9 0.4 shard_map.101
  17.3 13.5 %all-to-all-done.rows_ref = bf16[32,16,128]{2,1,0:T(8,128)(2,1)S(1)} async-done(((bf16[32,16,128]{2,1,0:T(8,128)(2,1)}), bf16[32,16,128]{2,1,0:T(8,128)(2,1)S(1)}, u32[]{:S(2)}, u32[]{:S(2)}) %all-to-all-start) | async-done | bytes 131104 | tf_op jit(solution)/shard_map/all_to_all | solution.py:245
  30.8 1.4 %shard_map.102 = (bf16[16,4096]{1,0:T(8,128)(2,1)}, bf16[1152,128]{1,0:T(8,128)(2,1)}) custom-call(bf16[32,16,128]{2,1,0:T(8,128)(2,1)S(1)} %all-to-all-done.rows_ref, f32[32,128]{1,0:T(8,128)S(1)} %get-tuple-element.16.gain_ref, bf16[40,16]{1,0:T(8,128)(2,1)S(1)} %get-tuple-element.19.select_ref), custom_call_target="tpu_custom_call" | custom-call | tf_op jit(solution)/shard_map/pallas_call | solution.py:189
  32.2 14.8 %all-to-all-start.1 = ((bf16[12,96,128]{2,1,0:T(8,128)(2,1)}), bf16[12,96,128]{2,1,0:T(8,128)(2,1)S(1)}, u32[]{:S(2)}, u32[]{:S(2)}) async-start(bf16[12,96,128]{2,1,0:T(8,128)(2,1)} %bitcast.11), calls=%async_computation.1 | async-start | bytes 589824 | tf_op jit(solution)/shard_map/all_to_all | solution.py:280
  47.0 0.0 collective-permute-done.g0
  47.0 3.2 %collective-permute-start.2 = (bf16[3,32,4096]{2,1,0:T(8,128)(2,1)S(1)}, bf16[3,32,4096]{2,1,0:T(8,128)(2,1)S(1)}, u32[]{:S(2)}, u32[]{:S(2)}) collective-permute-start(bf16[3,32,4096]{2,1,0:T(8,128)(2,1)S(1)} %collective-permute-done.g0), channel_id=1, source_target_pairs={{0,32},{32,0},{1,33},{33,1},{2,34},{34,2},{3,35},{35,3},{4,36},{36... | collective-permute-start | bytes 2359304 | tf_op jit(solution)/shard_map/ppermute | solution.py:263
  50.2 0.0 collective-permute-done.1.g1
  50.2 1.9 %collective-permute-start.3 = (bf16[3,32,4096]{2,1,0:T(8,128)(2,1)S(1)}, bf16[3,32,4096]{2,1,0:T(8,128)(2,1)S(1)}, u32[]{:S(2)}, u32[]{:S(2)}) collective-permute-start(bf16[3,32,4096]{2,1,0:T(8,128)(2,1)S(1)} %collective-permute-done.1.g1), channel_id=1, source_target_pairs={{0,32},{32,0},{1,33},{33,1},{2,34},{34,2},{3,35},{35,3},{4,36},{36... | collective-permute-start | bytes 2359304 | tf_op jit(solution)/shard_map/ppermute | solution.py:263
  52.1 12.9 %all-to-all-done.1 = bf16[12,96,128]{2,1,0:T(8,128)(2,1)S(1)} async-done(((bf16[12,96,128]{2,1,0:T(8,128)(2,1)}), bf16[12,96,128]{2,1,0:T(8,128)(2,1)S(1)}, u32[]{:S(2)}, u32[]{:S(2)}) %all-to-all-start.1) | async-done | bytes 294944 | tf_op jit(solution)/shard_map/all_to_all | solution.py:280
  65.0 0.0 collective-permute-done.2.g2
  65.0 0.0 collective-permute-done.3.g3
  65.0 2.2 %shard_map.103 = bf16[1152,128]{1,0:T(8,128)(2,1)} custom-call(bf16[1152,128]{1,0:T(8,128)(2,1)S(1)} %bitcast.9, bf16[3,32,4096]{2,1,0:T(8,128)(2,1)S(1)} %collective-permute-done.g0, bf16[3,32,4096]{2,1,0:T(8,128)(2,1)S(1)} %collective-permute-done.1.g1, bf16[3,32,4096]{2,1,0:T(8,128)(2,1)S(1)} %collective-permute-done.2.g2, ...), custom_call_target="tpu_custom_call" | custom-call | tf_op jit(solution)/shard_map/pallas_call | solution.py:189
  67.2 3.5 %all-to-all-start.2 = ((bf16[12,96,128]{2,1,0:T(8,128)(2,1)}), bf16[12,96,128]{2,1,0:T(8,128)(2,1)S(1)}, u32[]{:S(2)}, u32[]{:S(2)}) async-start(bf16[12,96,128]{2,1,0:T(8,128)(2,1)} %bitcast.7), calls=%async_computation.2 | async-start | bytes 589824 | tf_op jit(solution)/shard_map/all_to_all | solution.py:304
  70.7 2.4 %shard_map.104.shared_ref = f32[16,4096]{1,0:T(8,128)} custom-call(bf16[16,4096]{1,0:T(8,128)(2,1)} %get-tuple-element.24.own_ref, bf16[32,4096]{1,0:T(8,128)(2,1)} %gate_ref.3, bf16[32,4096]{1,0:T(8,128)(2,1)} %up_ref.3, bf16[32,4096]{1,0:T(8,128)(2,1)} %down_ref.3), custom_call_target="tpu_custom_call" | custom-call | tf_op jit(solution)/shard_map/pallas_call | solution.py:189
  73.0 14.5 %all-to-all-done.2 = bf16[12,96,128]{2,1,0:T(8,128)(2,1)S(1)} async-done(((bf16[12,96,128]{2,1,0:T(8,128)(2,1)}), bf16[12,96,128]{2,1,0:T(8,128)(2,1)S(1)}, u32[]{:S(2)}, u32[]{:S(2)}) %all-to-all-start.2) | async-done | bytes 294944 | tf_op jit(solution)/shard_map/all_to_all | solution.py:304
  87.5 0.0 copy-start
  87.5 0.9 copy-done
  88.5 0.5 shard_map.105
  89.0 14.8 %all_to_all.20.parts_ref = bf16[32,16,128]{2,1,0:T(8,128)(2,1)S(1)} all-to-all(bf16[32,16,128]{2,1,0:T(8,128)(2,1)S(1)} %shard_map.105), channel_id=1, replica_groups=mesh['z'=12,'c'=2,'y'=8,'x'=4] {'y','x'}, dimensions={0} | all-to-all | bytes 262144 | tf_op jit(solution)/shard_map/all_to_all | solution.py:314
  103.9 0.6 shard_map.106
Async XLA Ops:
  1.5 45.5 %collective-permute-start = (bf16[3,32,4096]{2,1,0:T(8,128)(2,1)S(1)}, bf16[3,32,4096]{2,1,0:T(8,128)(2,1)S(1)}, u32[]{:S(2)}, u32[]{:S(2)}) collective-permute-start(bf16[3,32,4096]{2,1,0:T(8,128)(2,1)S(1)} %get-tuple-element.21), channel_id=1, source_target_pairs={{0,1},{1,0},{2,3},{3,2},{4,33},{5,32},{6,35},{7,34},{8,9},{9,8},{1... | collective-permute-start | bytes 2359304 | tf_op jit(solution)/shard_map/ppermute | solution.py:262
  4.9 45.3 %collective-permute-start.1 = (bf16[3,32,4096]{2,1,0:T(8,128)(2,1)S(1)}, bf16[3,32,4096]{2,1,0:T(8,128)(2,1)S(1)}, u32[]{:S(2)}, u32[]{:S(2)}) collective-permute-start(bf16[3,32,4096]{2,1,0:T(8,128)(2,1)S(1)} %get-tuple-element.22), channel_id=1, source_target_pairs={{0,0},{1,1},{2,2},{3,3},{4,32},{5,33},{6,34},{7,35},{8,8},{9,9},{1... | collective-permute-start | bytes 2359304 | tf_op jit(solution)/shard_map/ppermute | solution.py:262
  5.6 25.1 %all-to-all-start = ((bf16[32,16,128]{2,1,0:T(8,128)(2,1)}), bf16[32,16,128]{2,1,0:T(8,128)(2,1)S(1)}, u32[]{:S(2)}, u32[]{:S(2)}) async-start(bf16[32,16,128]{2,1,0:T(8,128)(2,1)} %get-tuple-element.15), calls=%async_computation | async-start | bytes 262144 | tf_op jit(solution)/shard_map/all_to_all | solution.py:245
  32.2 32.8 %all-to-all-start.1 = ((bf16[12,96,128]{2,1,0:T(8,128)(2,1)}), bf16[12,96,128]{2,1,0:T(8,128)(2,1)S(1)}, u32[]{:S(2)}, u32[]{:S(2)}) async-start(bf16[12,96,128]{2,1,0:T(8,128)(2,1)} %bitcast.11), calls=%async_computation.1 | async-start | bytes 589824 | tf_op jit(solution)/shard_map/all_to_all | solution.py:280
  47.0 18.0 %collective-permute-start.2 = (bf16[3,32,4096]{2,1,0:T(8,128)(2,1)S(1)}, bf16[3,32,4096]{2,1,0:T(8,128)(2,1)S(1)}, u32[]{:S(2)}, u32[]{:S(2)}) collective-permute-start(bf16[3,32,4096]{2,1,0:T(8,128)(2,1)S(1)} %collective-permute-done.g0), channel_id=1, source_target_pairs={{0,32},{32,0},{1,33},{33,1},{2,34},{34,2},{3,35},{35,3},{4,36},{36... | collective-permute-start | bytes 2359304 | tf_op jit(solution)/shard_map/ppermute | solution.py:263
  50.2 14.8 %collective-permute-start.3 = (bf16[3,32,4096]{2,1,0:T(8,128)(2,1)S(1)}, bf16[3,32,4096]{2,1,0:T(8,128)(2,1)S(1)}, u32[]{:S(2)}, u32[]{:S(2)}) collective-permute-start(bf16[3,32,4096]{2,1,0:T(8,128)(2,1)S(1)} %collective-permute-done.1.g1), channel_id=1, source_target_pairs={{0,32},{32,0},{1,33},{33,1},{2,34},{34,2},{3,35},{35,3},{4,36},{36... | collective-permute-start | bytes 2359304 | tf_op jit(solution)/shard_map/ppermute | solution.py:263
  67.2 20.3 %all-to-all-start.2 = ((bf16[12,96,128]{2,1,0:T(8,128)(2,1)}), bf16[12,96,128]{2,1,0:T(8,128)(2,1)S(1)}, u32[]{:S(2)}, u32[]{:S(2)}) async-start(bf16[12,96,128]{2,1,0:T(8,128)(2,1)} %bitcast.7), calls=%async_computation.2 | async-start | bytes 589824 | tf_op jit(solution)/shard_map/all_to_all | solution.py:304
  87.5 1.0 copy-start

commit v7 on v6

--- a/solution.py
+++ b/solution.py
@@ -213,8 +213,7 @@
     shared_up,
     shared_down,
 ):
-    y, x = lax.axis_index("y"), lax.axis_index("x")
-    place = 2 * (y % 2) + x % 2
+    x = place = lax.axis_index("x")
     piece = shape((3, UNITS, N_TP * LANES))
     copies, take0, take1, across, weights, gain = call(
         first_body,
@@ -257,7 +256,7 @@
         for c in range(N_C):
             for j in range(N_TP):
                 sy, sx = j // N_X, j % N_X
-                target = (sy % 2) * N_TP + (sy - sy % 2 + c) * N_X + (sx - sx % 2 + (sx + 1 - m) % 2)
+                target = (sx // 2) * N_TP + sy * N_X + 2 * c + (sx + 1 - m) % 2
                 pairs.append((c * N_TP + j, target))
         mine.append(lax.ppermute(piece, ("c", "y", "x"), pairs))
         other.append(lax.ppermute(mine[-1], "c", [(0, 1), (1, 0)]))

time: 105 us -> 104 us (level)
  the two profiles are of different devices: /device:TPU:64 before, /device:TPU:1 now
where the time goes in v7:
time: 104 us; the launch traced here: 102 us
  starting transfers between devices  45.7 us (44%)
  waiting for transfers between devices  24 us (23%)
  blocking collectives  22.2 us (21%)
  Pallas kernels  9.04 us (9%)
    all_to_all x1, blocking collectives, per_device(): mixed = lax.all_to_all(mixed, ('y', 'x'), 0, 0, tiled=True)  22.2 us
    all_to_all x1, starting transfers between devices, per_device(): lax.all_to_all(packed.reshape(N_Z, CAP * N_TP, LANES), 'z', 0, 0, tiled=T...  14.9 us
    all_to_all x1, waiting for transfers between devices, per_device(): lax.all_to_all(parts.reshape(N_Z, CAP * N_TP, LANES), 'z', 0, 0, tiled=True)  10.6 us
    all_to_all x1, waiting for transfers between devices, per_device(): tokens = lax.all_to_all(copies, ('y', 'x'), 0, 0, tiled=True)  9.11 us
    pallas_call x7, Pallas kernels, call(): pl.pallas_call(body, in_specs=ins, out_specs=outspecs or [VMEM] * len(sha...  9.04 us
    ppermute x2, starting transfers between devices, per_device(): other.append(lax.ppermute(mine[-1], 'c', [(0, 1), (1, 0)]))  8.32 us
    ppermute x2, starting transfers between devices, per_device(): mine.append(lax.ppermute(piece, ('c', 'y', 'x'), pairs))  7.95 us
    all_to_all x1, starting transfers between devices, per_device(): lax.all_to_all(parts.reshape(N_Z, CAP * N_TP, LANES), 'z', 0, 0, tiled=True)  7.33 us
  transfers between devices with their start and end apart: 7, of which 3 were waited for; matrix products, arithmetic and copies ran while one was open for 0% of the time, Pallas kernels for 4%

profile of v7, /device:TPU:1, one launch (start us, length us, event | category | flops | bytes accessed | tf_op | source)
XLA Modules:
  0.0 102.1 jit_solution(4827278071758680576)
XLA Ops:
  0.0 1.5 %shard_map.100 = (bf16[32,16,128]{2,1,0:T(8,128)(2,1)}, bf16[3,32,4096]{2,1,0:T(8,128)(2,1)S(1)}, bf16[3,32,4096]{2,1,0:T(8,128)(2,1)S(1)}, s32[4,16]{1,0:T(4,12...) custom-call(s32[1]{0:T(128)} %bitcast.bit_ref, bf16[16,128]{1,0:T(8,128)(2,1)} %hidden_ref.1, ...), custom_call_target="tpu_custom_call" | custom-call | tf_op jit(solution)/shard_map/pallas_call | solution.py:189
  1.5 5.8 %collective-permute-start = (bf16[3,32,4096]{2,1,0:T(8,128)(2,1)S(1)}, bf16[3,32,4096]{2,1,0:T(8,128)(2,1)S(1)}, u32[]{:S(2)}, u32[]{:S(2)}) collective-permute-start(bf16[3,32,4096]{2,1,0:T(8,128)(2,1)S(1)} %get-tuple-element.21), channel_id=1, source_target_pairs={{0,1},{1,0},{2,33},{3,32},{4,5},{5,4},{6,37},{7,36},{8,9},{9,8},{1... | collective-permute-start | bytes 2359304 | tf_op jit(solution)/shard_map/ppermute | solution.py:261
  7.3 2.2 %collective-permute-start.1 = (bf16[3,32,4096]{2,1,0:T(8,128)(2,1)S(1)}, bf16[3,32,4096]{2,1,0:T(8,128)(2,1)S(1)}, u32[]{:S(2)}, u32[]{:S(2)}) collective-permute-start(bf16[3,32,4096]{2,1,0:T(8,128)(2,1)S(1)} %get-tuple-element.22), channel_id=1, source_target_pairs={{0,0},{1,1},{2,32},{3,33},{4,4},{5,5},{6,36},{7,37},{8,8},{9,9},{1... | collective-permute-start | bytes 2359304 | tf_op jit(solution)/shard_map/ppermute | solution.py:261
  9.5 7.2 %all-to-all-start = ((bf16[32,16,128]{2,1,0:T(8,128)(2,1)}), bf16[32,16,128]{2,1,0:T(8,128)(2,1)S(1)}, u32[]{:S(2)}, u32[]{:S(2)}) async-start(bf16[32,16,128]{2,1,0:T(8,128)(2,1)} %get-tuple-element.15), calls=%async_computation | async-start | bytes 262144 | tf_op jit(solution)/shard_map/all_to_all | solution.py:244
  16.7 0.4 shard_map.101
  17.1 9.1 %all-to-all-done.rows_ref = bf16[32,16,128]{2,1,0:T(8,128)(2,1)S(1)} async-done(((bf16[32,16,128]{2,1,0:T(8,128)(2,1)}), bf16[32,16,128]{2,1,0:T(8,128)(2,1)S(1)}, u32[]{:S(2)}, u32[]{:S(2)}) %all-to-all-start) | async-done | bytes 131104 | tf_op jit(solution)/shard_map/all_to_all | solution.py:244
  26.2 1.4 %shard_map.102 = (bf16[16,4096]{1,0:T(8,128)(2,1)}, bf16[1152,128]{1,0:T(8,128)(2,1)}) custom-call(bf16[32,16,128]{2,1,0:T(8,128)(2,1)S(1)} %all-to-all-done.rows_ref, f32[32,128]{1,0:T(8,128)S(1)} %get-tuple-element.16.gain_ref, bf16[40,16]{1,0:T(8,128)(2,1)S(1)} %get-tuple-element.19.select_ref), custom_call_target="tpu_custom_call" | custom-call | tf_op jit(solution)/shard_map/pallas_call | solution.py:189
  27.7 14.9 %all-to-all-start.1 = ((bf16[12,96,128]{2,1,0:T(8,128)(2,1)}), bf16[12,96,128]{2,1,0:T(8,128)(2,1)S(1)}, u32[]{:S(2)}, u32[]{:S(2)}) async-start(bf16[12,96,128]{2,1,0:T(8,128)(2,1)} %bitcast.11), calls=%async_computation.1 | async-start | bytes 589824 | tf_op jit(solution)/shard_map/all_to_all | solution.py:279
  42.6 0.0 collective-permute-done.g0
  42.6 6.4 %collective-permute-start.2 = (bf16[3,32,4096]{2,1,0:T(8,128)(2,1)S(1)}, bf16[3,32,4096]{2,1,0:T(8,128)(2,1)S(1)}, u32[]{:S(2)}, u32[]{:S(2)}) collective-permute-start(bf16[3,32,4096]{2,1,0:T(8,128)(2,1)S(1)} %collective-permute-done.g0), channel_id=1, source_target_pairs={{0,32},{32,0},{1,33},{33,1},{2,34},{34,2},{3,35},{35,3},{4,36},{36... | collective-permute-start | bytes 2359304 | tf_op jit(solution)/shard_map/ppermute | solution.py:262
  49.0 0.0 collective-permute-done.1.g1
  49.0 1.9 %collective-permute-start.3 = (bf16[3,32,4096]{2,1,0:T(8,128)(2,1)S(1)}, bf16[3,32,4096]{2,1,0:T(8,128)(2,1)S(1)}, u32[]{:S(2)}, u32[]{:S(2)}) collective-permute-start(bf16[3,32,4096]{2,1,0:T(8,128)(2,1)S(1)} %collective-permute-done.1.g1), channel_id=1, source_target_pairs={{0,32},{32,0},{1,33},{33,1},{2,34},{34,2},{3,35},{35,3},{4,36},{36... | collective-permute-start | bytes 2359304 | tf_op jit(solution)/shard_map/ppermute | solution.py:262
  50.9 4.2 %all-to-all-done.1 = bf16[12,96,128]{2,1,0:T(8,128)(2,1)S(1)} async-done(((bf16[12,96,128]{2,1,0:T(8,128)(2,1)}), bf16[12,96,128]{2,1,0:T(8,128)(2,1)S(1)}, u32[]{:S(2)}, u32[]{:S(2)}) %all-to-all-start.1) | async-done | bytes 294944 | tf_op jit(solution)/shard_map/all_to_all | solution.py:279
  55.2 0.0 collective-permute-done.2.g2
  55.2 0.0 collective-permute-done.3.g3
  55.2 2.2 %shard_map.103 = bf16[1152,128]{1,0:T(8,128)(2,1)} custom-call(bf16[1152,128]{1,0:T(8,128)(2,1)S(1)} %bitcast.9, bf16[3,32,4096]{2,1,0:T(8,128)(2,1)S(1)} %collective-permute-done.g0, bf16[3,32,4096]{2,1,0:T(8,128)(2,1)S(1)} %collective-permute-done.1.g1, bf16[3,32,4096]{2,1,0:T(8,128)(2,1)S(1)} %collective-permute-done.2.g2, ...), custom_call_target="tpu_custom_call" | custom-call | tf_op jit(solution)/shard_map/pallas_call | solution.py:189
  57.4 7.3 %all-to-all-start.2 = ((bf16[12,96,128]{2,1,0:T(8,128)(2,1)}), bf16[12,96,128]{2,1,0:T(8,128)(2,1)S(1)}, u32[]{:S(2)}, u32[]{:S(2)}) async-start(bf16[12,96,128]{2,1,0:T(8,128)(2,1)} %bitcast.7), calls=%async_computation.2 | async-start | bytes 589824 | tf_op jit(solution)/shard_map/all_to_all | solution.py:303
  64.7 2.4 %shard_map.104.shared_ref = f32[16,4096]{1,0:T(8,128)} custom-call(bf16[16,4096]{1,0:T(8,128)(2,1)} %get-tuple-element.24.own_ref, bf16[32,4096]{1,0:T(8,128)(2,1)} %gate_ref.3, bf16[32,4096]{1,0:T(8,128)(2,1)} %up_ref.3, bf16[32,4096]{1,0:T(8,128)(2,1)} %down_ref.3), custom_call_target="tpu_custom_call" | custom-call | tf_op jit(solution)/shard_map/pallas_call | solution.py:189
  67.1 10.6 %all-to-all-done.2 = bf16[12,96,128]{2,1,0:T(8,128)(2,1)S(1)} async-done(((bf16[12,96,128]{2,1,0:T(8,128)(2,1)}), bf16[12,96,128]{2,1,0:T(8,128)(2,1)S(1)}, u32[]{:S(2)}, u32[]{:S(2)}) %all-to-all-start.2) | async-done | bytes 294944 | tf_op jit(solution)/shard_map/all_to_all | solution.py:303
  77.7 0.0 copy-start
  77.7 0.9 copy-done
  78.6 0.5 shard_map.105
  79.2 22.2 %all_to_all.20.parts_ref = bf16[32,16,128]{2,1,0:T(8,128)(2,1)S(1)} all-to-all(bf16[32,16,128]{2,1,0:T(8,128)(2,1)S(1)} %shard_map.105), channel_id=1, replica_groups=mesh['z'=12,'c'=2,'y'=8,'x'=4] {'y','x'}, dimensions={0} | all-to-all | bytes 262144 | tf_op jit(solution)/shard_map/all_to_all | solution.py:313
  101.4 0.6 shard_map.106
Async XLA Ops:
  1.5 41.1 %collective-permute-start = (bf16[3,32,4096]{2,1,0:T(8,128)(2,1)S(1)}, bf16[3,32,4096]{2,1,0:T(8,128)(2,1)S(1)}, u32[]{:S(2)}, u32[]{:S(2)}) collective-permute-start(bf16[3,32,4096]{2,1,0:T(8,128)(2,1)S(1)} %get-tuple-element.21), channel_id=1, source_target_pairs={{0,1},{1,0},{2,33},{3,32},{4,5},{5,4},{6,37},{7,36},{8,9},{9,8},{1... | collective-permute-start | bytes 2359304 | tf_op jit(solution)/shard_map/ppermute | solution.py:261
  7.3 41.7 %collective-permute-start.1 = (bf16[3,32,4096]{2,1,0:T(8,128)(2,1)S(1)}, bf16[3,32,4096]{2,1,0:T(8,128)(2,1)S(1)}, u32[]{:S(2)}, u32[]{:S(2)}) collective-permute-start(bf16[3,32,4096]{2,1,0:T(8,128)(2,1)S(1)} %get-tuple-element.22), channel_id=1, source_target_pairs={{0,0},{1,1},{2,32},{3,33},{4,4},{5,5},{6,36},{7,37},{8,8},{9,9},{1... | collective-permute-start | bytes 2359304 | tf_op jit(solution)/shard_map/ppermute | solution.py:261
  9.5 16.7 %all-to-all-start = ((bf16[32,16,128]{2,1,0:T(8,128)(2,1)}), bf16[32,16,128]{2,1,0:T(8,128)(2,1)S(1)}, u32[]{:S(2)}, u32[]{:S(2)}) async-start(bf16[32,16,128]{2,1,0:T(8,128)(2,1)} %get-tuple-element.15), calls=%async_computation | async-start | bytes 262144 | tf_op jit(solution)/shard_map/all_to_all | solution.py:244
  27.7 27.5 %all-to-all-start.1 = ((bf16[12,96,128]{2,1,0:T(8,128)(2,1)}), bf16[12,96,128]{2,1,0:T(8,128)(2,1)S(1)}, u32[]{:S(2)}, u32[]{:S(2)}) async-start(bf16[12,96,128]{2,1,0:T(8,128)(2,1)} %bitcast.11), calls=%async_computation.1 | async-start | bytes 589824 | tf_op jit(solution)/shard_map/all_to_all | solution.py:279
  42.6 12.6 %collective-permute-start.2 = (bf16[3,32,4096]{2,1,0:T(8,128)(2,1)S(1)}, bf16[3,32,4096]{2,1,0:T(8,128)(2,1)S(1)}, u32[]{:S(2)}, u32[]{:S(2)}) collective-permute-start(bf16[3,32,4096]{2,1,0:T(8,128)(2,1)S(1)} %collective-permute-done.g0), channel_id=1, source_target_pairs={{0,32},{32,0},{1,33},{33,1},{2,34},{34,2},{3,35},{35,3},{4,36},{36... | collective-permute-start | bytes 2359304 | tf_op jit(solution)/shard_map/ppermute | solution.py:262
  49.0 6.2 %collective-permute-start.3 = (bf16[3,32,4096]{2,1,0:T(8,128)(2,1)S(1)}, bf16[3,32,4096]{2,1,0:T(8,128)(2,1)S(1)}, u32[]{:S(2)}, u32[]{:S(2)}) collective-permute-start(bf16[3,32,4096]{2,1,0:T(8,128)(2,1)S(1)} %collective-permute-done.1.g1), channel_id=1, source_target_pairs={{0,32},{32,0},{1,33},{33,1},{2,34},{34,2},{3,35},{35,3},{4,36},{36... | collective-permute-start | bytes 2359304 | tf_op jit(solution)/shard_map/ppermute | solution.py:262
  57.4 20.3 %all-to-all-start.2 = ((bf16[12,96,128]{2,1,0:T(8,128)(2,1)}), bf16[12,96,128]{2,1,0:T(8,128)(2,1)S(1)}, u32[]{:S(2)}, u32[]{:S(2)}) async-start(bf16[12,96,128]{2,1,0:T(8,128)(2,1)} %bitcast.7), calls=%async_computation.2 | async-start | bytes 589824 | tf_op jit(solution)/shard_map/all_to_all | solution.py:303
  77.7 1.0 copy-start
